TPU v7x, 32 devices: a whole 2x2x4 slice. The times are simulated.
32 devices in a mesh: grp: 2 (over y), ep: 4 (over z), tp: 4 (over x, core).
Axes of the slice: x: 2, y: 2, z: 4, core: 2. Of those that a mesh axis runs over, the one named last changes fastest.
Arguments:
- mix_query: bfloat16 [4096, 16, 128], P(('grp', 'ep'), 'tp'), parts along dimension 0, may hold values from -6 to 6
- mix_keys: bfloat16 [4096, 16, 128], P(('grp', 'ep'), 'tp'), parts along dimension 0, may hold values from -6 to 6
- mix_values: bfloat16 [4096, 16, 128], P(('grp', 'ep'), 'tp'), parts along dimension 0, may hold values from -6 to 6
- beta_in: float32 [16, 4096], P('tp', ('grp', 'ep')), parts along dimension 1, may hold values from -9.5 to 6
- decay_in: float32 [16, 4096], P('tp', ('grp', 'ep')), parts along dimension 1, may hold values from -14 to 0
- norm_gain: float32 [128], replicated, may hold values from 0.1 to 1.9
- ffn_input: bfloat16 [1024, 4096], P(('grp', 'ep'), 'tp'), parts along dimension 0, may hold values from -200 to 200
- ffn_gain: float32 [4096], P('tp'), may hold values from 0.1 to 1.9
- expert_ids: int32 [1024, 2], P(('grp', 'ep')), parts along dimension 0, may hold values from 0 to 15, as said below
- expert_share: float32 [1024, 2], P(('grp', 'ep')), parts along dimension 0, may hold values from 0.2 to 1
- w_gate: bfloat16 [16, 4096, 1024], P('ep', None, 'tp'), may hold values from -0.09375 to 0.09375
- w_up: bfloat16 [16, 4096, 1024], P('ep', None, 'tp'), may hold values from -0.09375 to 0.09375
- w_down: bfloat16 [16, 1024, 4096], P('ep', None, 'tp'), may hold values from -0.1875 to 0.1875
Outputs:
- mix_out: bfloat16 [4096, 16, 128], P(('grp', 'ep'), 'tp'), parts along dimension 0
- ffn_out: bfloat16 [1024, 4096], P(('grp', 'ep'), 'tp'), parts along dimension 0
There are 2 independent parts, one for each index of `grp`. A program takes and returns all parts, laid end to end along the dimension named above; an argument that names none is the same for every part. Nothing has to cross between parts.
Inputs may be any that keep to these rules, and one draw needn't show every extreme that they name: `expert_ids`: each row names two different experts of one group, the group being id // 4; the rows of one device (aligned blocks of 128 rows) name every expert exactly 2 * 128 // 16 times.
All inputs are finite; a program needn't handle non-finite values.
Results may differ from a plain program's by a relative error of at most 0.007.
Values may be sent and summed in bfloat16 or wider, within the bound.
A program may use at most 128 MiB of HBM per device.

v0:
```python
import functools
import jax
import jax.numpy as jnp
from jax import lax
from jax.experimental import pallas as pl
from jax.experimental.pallas import tpu as pltpu
from jax.sharding import PartitionSpec as P

BLOCK = 64
GROUP = 4
F32 = jnp.float32
BF16 = jnp.bfloat16
MESH = pl.DeviceIdType.MESH
ROWS_COLS = (((1,), (0,)), ((), ()))
ROWS_ROWS = (((1,), (1,)), ((), ()))
COLS_COLS = (((0,), (0,)), ((), ()))


PRECISE = lax.Precision.HIGHEST
EPSILON = 1e-06


def entering_2(value, axis, join, neutral):
    count, mine = (lax.axis_size(axis), lax.axis_index(axis))
    pieces = jax.tree.map(lambda part: lax.all_gather(part, axis), value)
    subtotal = jax.tree.map(
        lambda part, zero: jnp.full_like(part, 0) + jnp.asarray(zero, part.dtype), value, neutral
    )

    def turn(position, subtotal):
        longer = join(subtotal, jax.tree.map(lambda part: part[position], pieces))
        return jax.tree.map(lambda new, old: jnp.where(position < mine, new, old), longer, subtotal)

    return lax.fori_loop(0, count - 1, turn, subtotal)


def unit_inverse(strict_lower):
    extent = strict_lower.shape[-1]
    identity = jnp.eye(extent, dtype=jnp.float32)
    powered = -strict_lower
    product = identity + powered
    for section_index in range(1, (extent - 1).bit_length()):
        powered = jnp.matmul(powered, powered, precision=PRECISE)
        product = jnp.matmul(product, identity + powered, precision=PRECISE)
    return product


def block_terms(queries, keyset, valueset, betas, rates):
    extent = queries.shape[-2]
    cumulative = -jnp.cumsum(rates, axis=-1)
    positions = jnp.arange(extent)
    causal = positions[:, None] >= positions[None, :]
    strict = positions[:, None] > positions[None, :]
    spread = cumulative[..., :, None] - cumulative[..., None, :]
    decay_mask = jnp.where(causal, jnp.exp(jnp.where(causal, spread, 0.0)), 0.0)
    keys_beta = keyset * betas[..., None]
    values_beta = valueset * betas[..., None]
    lower_part = jnp.where(
        strict,
        jnp.einsum("...id,...jd->...ij", keys_beta, keyset, precision=PRECISE) * decay_mask,
        0.0,
    )
    inverse = unit_inverse(lower_part)
    update = jnp.einsum("...ij,...jd->...id", inverse, values_beta, precision=PRECISE)
    correction = jnp.einsum(
        "...ij,...jd->...id", inverse, keys_beta * jnp.exp(cumulative)[..., None], precision=PRECISE
    )
    scores = jnp.where(
        causal,
        jnp.einsum("...id,...jd->...ij", queries, keyset, precision=PRECISE) * decay_mask,
        0.0,
    )
    query_decay = queries * jnp.exp(cumulative)[..., None]
    key_decay = keyset * jnp.exp(cumulative[..., -1:] - cumulative)[..., None]
    block_decay = jnp.exp(cumulative[..., -1])
    return (query_decay, key_decay, update, correction, scores, block_decay)


def unit_rows(values_in, factor):
    floats = values_in.astype(jnp.float32)
    return floats * lax.rsqrt(jnp.sum(floats * floats, -1, keepdims=True) + EPSILON) * factor


def compose(earlier, later):
    return (
        jnp.matmul(later[0], earlier[0], precision=PRECISE),
        jnp.matmul(later[0], earlier[1], precision=PRECISE) + later[1],
    )


def mixer_body(mix_query, mix_keys, mix_values, beta_in, decay_in, norm_gain):
    length, head_count, width = mix_query.shape
    blocks = length // BLOCK

    def to_blocks(tensor):
        return tensor.reshape(blocks, BLOCK, head_count, width).transpose(2, 0, 1, 3)

    queries = to_blocks(unit_rows(mix_query, width ** (-0.5)))
    keyset = to_blocks(unit_rows(mix_keys, 1.0))
    valueset = to_blocks(mix_values.astype(jnp.float32))
    betas = jax.nn.sigmoid(beta_in).reshape(head_count, blocks, BLOCK)
    rates = jax.nn.softplus(decay_in).reshape(head_count, blocks, BLOCK)
    query_decay, key_decay, update, correction, scores, block_decay = block_terms(
        queries, keyset, valueset, betas, rates
    )
    identity = jnp.eye(width, dtype=jnp.float32)
    transfer = block_decay[..., None, None] * identity - jnp.einsum(
        "hncd,hnce->hnde", key_decay, correction, precision=PRECISE
    )
    offset = jnp.einsum("hncd,hnce->hnde", key_decay, update, precision=PRECISE)
    prefix_map, prefix_add = lax.associative_scan(compose, (transfer, offset), axis=1)
    total_map = prefix_map[:, -1]
    total_add = prefix_add[:, -1]
    empty_state = jnp.zeros((head_count, width, width), jnp.float32)
    unit_maps = jnp.broadcast_to(identity, (head_count, width, width))
    ignored_map, entering = entering_2(
        (total_map, total_add), "ep", compose, (unit_maps, empty_state)
    )
    after_blocks = jnp.matmul(prefix_map, entering[:, None], precision=PRECISE) + prefix_add
    starts = jnp.concatenate([entering[:, None], after_blocks[:, :-1]], axis=1)
    fresh = update - jnp.einsum("hncd,hnde->hnce", correction, starts, precision=PRECISE)
    outputs = jnp.einsum("hncd,hnde->hnce", query_decay, starts, precision=PRECISE) + jnp.einsum(
        "hnij,hnje->hnie", scores, fresh, precision=PRECISE
    )
    raw_mix = outputs.transpose(1, 2, 0, 3).reshape(length, head_count, width)
    return (
        raw_mix * lax.rsqrt(jnp.mean(raw_mix * raw_mix, -1, keepdims=True) + EPSILON) * norm_gain
    ).astype(jnp.bfloat16)


def experts_body(ffn_input, ffn_gain, expert_ids, expert_share, w_gate, w_up, w_down):
    floats = ffn_input.astype(jnp.float32)
    square_sum = lax.psum(jnp.sum(floats * floats, -1), "tp")
    full_width = ffn_input.shape[1] * lax.axis_size("tp")
    normed = (floats * lax.rsqrt(square_sum / full_width + EPSILON)[:, None] * ffn_gain).astype(
        jnp.bfloat16
    )
    pick_count = expert_ids.shape[1]
    flat_ids = expert_ids.reshape(-1)
    sort_order = jnp.argsort(flat_ids, stable=True)
    source_rows = sort_order // pick_count
    experts_local = w_gate.shape[0]
    expert_devices = lax.axis_size("ep")
    capacity = flat_ids.shape[0] // (experts_local * expert_devices)
    outgoing = normed[source_rows].reshape(expert_devices, experts_local, capacity, normed.shape[1])
    arrived = lax.all_to_all(outgoing, "ep", split_axis=0, concat_axis=0, tiled=True)
    slab_in = lax.all_gather(arrived, "tp", axis=3, tiled=True)
    gate_sum = jnp.einsum("secl,elf->secf", slab_in, w_gate, preferred_element_type=jnp.float32)
    up_sum = jnp.einsum("secl,elf->secf", slab_in, w_up, preferred_element_type=jnp.float32)
    hidden = (jax.nn.silu(gate_sum) * up_sum).astype(jnp.bfloat16)
    merged = jnp.einsum(
        "secf,efd->secd",
        lax.all_gather(hidden, "tp", axis=3, tiled=True),
        w_down,
        preferred_element_type=jnp.float32,
    )
    copies = merged.astype(jnp.bfloat16)
    returned = lax.all_to_all(copies, "ep", split_axis=0, concat_axis=0, tiled=True).reshape(
        -1, w_down.shape[2]
    )
    slots = jnp.argsort(sort_order)
    per_slot = returned[slots].reshape(expert_ids.shape[0], pick_count, -1)
    return jnp.sum(per_slot.astype(jnp.float32) * expert_share[..., None], axis=1).astype(
        jnp.bfloat16
    )

def mm(a, b, dims=ROWS_COLS):
    return lax.dot_general(a, b, dims, preferred_element_type=F32)


def exact(a, b, dims=ROWS_COLS):
    return lax.dot_general(a, b, dims, preferred_element_type=F32, precision=PRECISE)


def halves(a):
    high = a.astype(BF16)
    return high, (a - high.astype(F32)).astype(BF16)


def dot3(a, b):
    ah, al = halves(a)
    bh, bl = halves(b)
    return mm(ah, bh) + mm(ah, bl) + mm(al, bh)


def iota(shape, dim):
    return lax.broadcasted_iota(jnp.int32, shape, dim)


def flipped(row, n):
    return jnp.transpose(jnp.broadcast_to(row, (n, n)))


def decays(h, here, k, cum_s):
    n = k.shape[0]
    kf = k.astype(F32)
    rk = lax.rsqrt(jnp.sum(kf * kf, -1, keepdims=True) + EPSILON)
    rk_t = jnp.transpose(jnp.broadcast_to(rk, (n, n)))
    crow = cum_s[h, :, here]
    ccol = flipped(crow, n)
    causal = iota((n, n), 0) >= iota((n, n), 1)
    dm = jnp.where(causal, jnp.exp(jnp.where(causal, ccol - crow, 0.0)), 0.0) * rk_t
    return rk, rk_t, crow, ccol, dm


def state_part(h, k_ref, v_ref, cum_s, beta_s, wu_s, z_s, m_s, n_s, service):
    length = k_ref.shape[0]
    n = 128
    chunks = range(length // n)
    lanes = pl.ds(pl.multiple_of(h * n, n), n)
    row, col = iota((n, n), 0), iota((n, n), 1)
    strict = row > col
    same = (row >= n // 2) == (col >= n // 2)
    eye = (row == col).astype(F32)
    prods, powers, offs, tails, rowsets = [], [], [], [], []
    for c in chunks:
        here = slice(c * n, (c + 1) * n)
        k = k_ref[here, lanes]
        rk, rk_t, crow, ccol, dm = decays(h, here, k, cum_s)
        brow = beta_s[h, :, here]
        bcol = flipped(brow, n)
        lower = jnp.where(strict, mm(k, k, ROWS_ROWS) * dm * (rk * bcol), 0.0)
        neg = jnp.where(same, -lower, 0.0)
        offs.append(jnp.where(same, 0.0, lower))
        prods.append(eye + neg)
        powers.append(neg)
        clast = crow[:, n - 1 :]
        tails.append((rk * jnp.exp(clast - ccol), jnp.exp(clast)))
        rowsets.append((brow, brow * rk_t * jnp.exp(crow)))
    powers = [dot3(p, p) for p in powers]
    for turn in range((BLOCK - 1).bit_length() - 2):
        both = [dot3(jnp.concatenate([a, p], 0), p) for a, p in zip(prods, powers)]
        prods = [a + b[:n] for a, b in zip(prods, both)]
        powers = [b[n:] for b in both]
        if turn == 1:
            service()
    prods = [a + dot3(a, p) for a, p in zip(prods, powers)]
    mids = [dot3(o, a) for o, a in zip(offs, prods)]
    prods = [a - dot3(a, m) for a, m in zip(prods, mids)]
    pairs = []
    for c in chunks:
        here = slice(c * n, (c + 1) * n)
        uh, ul = halves(prods[c] * rowsets[c][0])
        wh, wl = halves(prods[c] * rowsets[c][1])
        k, v = k_ref[here, lanes], v_ref[here, lanes]
        pairs.append(jnp.concatenate([mm(wh, k) + mm(wl, k), mm(uh, v) + mm(ul, v)], 1))
        wu_s[h, here, :] = pairs[c]
    state = None
    for c in chunks:
        here = slice(c * n, (c + 1) * n)
        scale, last = tails[c]
        sh, sl = halves(pairs[c] * jnp.concatenate([scale, scale], 1))
        k = k_ref[here, lanes]
        moved = mm(k, sh, COLS_COLS) + mm(k, sl, COLS_COLS)
        step, add = last * eye - moved[:, :n], moved[:, n:]
        if state is None:
            state = jnp.concatenate([step, add], 1)
        else:
            z_s[h, c - 1] = state
            state = dot3(step, state) + jnp.concatenate([jnp.zeros_like(add), add], 1)
    m_s[h] = state[:, :n]
    n_s[h] = state[:, n:]


def output_part(h, q_ref, k_ref, cum_s, wu_s, z_s, gp_s, y_s):
    length = q_ref.shape[0]
    n = 128
    lanes = pl.ds(pl.multiple_of(h * n, n), n)
    chunks = range(length // n)
    spreads, qds = [], []
    for c in chunks:
        here = slice(c * n, (c + 1) * n)
        q, k = q_ref[here, lanes], k_ref[here, lanes]
        qf = q.astype(F32)
        rq = lax.rsqrt(jnp.sum(qf * qf, -1, keepdims=True) + EPSILON) * (n ** (-0.5))
        _, _, _, ccol, dm = decays(h, here, k, cum_s)
        spreads.append(dot3(mm(q, k, ROWS_ROWS) * dm * rq, wu_s[h, here, :]))
        qds.append(qf * rq * jnp.exp(ccol))
    for c in chunks:
        here = slice(c * n, (c + 1) * n)
        reader, base = qds[c] - spreads[c][:, :n], spreads[c][:, n:]
        if c == 0:
            gp_s[h, here, :] = reader
            y_s[h, here, :] = base
        else:
            both = dot3(reader, z_s[h, c - 1])
            gp_s[h, here, :] = both[:, :n]
            y_s[h, here, :] = both[:, n:] + base


def layer_kernel(
    q_ref, k_ref, v_ref, beta_ref, decay_ref, ngain_ref, x_ref, gain_ref, ids_ref, share_ref,
    wg_ref, wu_ref, wd_ref, mix_ref, ffn_ref,
    q_s, k_s, v_s, rows_s, wu_s, z_s, cum_s, beta_s, gp_s, y_s, m_s, n_s, sin_s, sout_s,
    wg_v, wu_v, wd_v, perm_s, disp, info_out, info_all, gall, xall, xe, hmine, hall, place_s, back_s, wide_s, copies_s,
    ret_out, ret_in,
    w_sem, d_send, d_recv, i_send, i_recv, g_send, g_recv,
    gx_send, gx_recv, gc_send, gc_recv, hx_send, hx_recv, hc_send, hc_recv,
    r_send, r_recv, c_send, c_recv,
):
    ep, tp = lax.axis_size("ep"), lax.axis_size("tp")
    me, mt = lax.axis_index("ep"), lax.axis_index("tp")
    chips = tp // 2
    chip, core = mt // 2, lax.rem(mt, 2)
    mate = chip * 2 + 1 - core
    heads, length = beta_ref.shape
    tokens, dl = x_ref.shape
    local = wg_ref.shape[0]
    cap = tokens // ep
    cap_e = tokens * 2 // local
    parts = r_send.shape[1]
    wide_part = ffn_ref.shape[1] // parts

    def away(axis, count, mine, step):
        return {axis: lax.rem(mine + step, count)}

    def remote(src, dst, ssem, rsem, device):
        return pltpu.make_async_remote_copy(
            src_ref=src, dst_ref=dst, send_sem=ssem, recv_sem=rsem,
            device_id=device, device_id_type=MESH,
        )

    barrier = pltpu.get_barrier_semaphore()
    for step in range(1, ep):
        pl.semaphore_signal(barrier, inc=1, device_id=away("ep", ep, me, step), device_id_type=MESH)
    for step in range(1, tp):
        pl.semaphore_signal(barrier, inc=1, device_id=away("tp", tp, mt, step), device_id_type=MESH)

    def weight(which, e):
        src, dst = ((wg_ref, wg_v), (wu_ref, wu_v), (wd_ref, wd_v))[which]
        return pltpu.make_async_copy(src.at[e], dst.at[e], w_sem.at[which, e])

    for which in range(3):
        for e in range(local):
            weight(which, e).start()

    ids = ids_ref[...]
    first = ids[0:1]
    group = jnp.zeros_like(first)
    for d in range(1, ep):
        group = group + (first >= d * local).astype(jnp.int32)
    n_rows = info_out.shape[0]
    upper = (iota((tokens, tokens), 0) < iota((tokens, tokens), 1)).astype(F32).astype(BF16)
    g_rows = max(8, ep)
    member = (iota((g_rows, tokens), 0) == group).astype(F32)
    rank = jnp.sum(member * mm(member.astype(BF16), upper), 0, keepdims=True)
    slot = group.astype(F32) * cap + rank
    perm = (iota((tokens, tokens), 0).astype(F32) == slot).astype(F32)
    perm_s[...] = perm.astype(BF16)
    disp[...] = mm(perm.astype(BF16), x_ref[...]).astype(BF16)
    l0, l1 = ids[0:1] - group * local, ids[1:2] - group * local
    shares = share_ref[...]
    line = iota((n_rows, tokens), 0)
    picked = ((line == l0) | (line == l1)).astype(F32)
    shared = jnp.where(
        line - local == l0, shares[0:1], jnp.where(line - local == l1, shares[1:2], 0.0)
    )
    info = exact(jnp.where(line < local, picked, shared), perm, ROWS_ROWS)
    info_out[...] = info
    info_all[me] = info
    gall[mt] = gain_ref[...]
    xall[mt, pl.ds(pl.multiple_of(me * cap, cap), cap), :] = disp[
        pl.ds(pl.multiple_of(me * cap, cap), cap), :
    ]

    def dispatch(step):
        to = lax.rem(me + step, ep)
        return remote(
            disp.at[pl.ds(pl.multiple_of(to * cap, cap), cap)],
            xall.at[mt, pl.ds(pl.multiple_of(me * cap, cap), cap)],
            d_send.at[to], d_recv.at[me], {"ep": to},
        )

    def tell(step):
        to = lax.rem(me + step, ep)
        return remote(info_out, info_all.at[me], i_send.at[to], i_recv.at[me], {"ep": to})

    def gains(step):
        to = lax.rem(mt + step, tp)
        return remote(gain_ref, gall.at[mt], g_send.at[to], g_recv.at[mt], {"tp": to})

    def chunk_of(origin, s):
        return xall.at[origin, pl.ds(pl.multiple_of(s * cap, cap), cap)]

    def over_x(step, s):
        to = lax.rem(chip + step, chips)
        part = chunk_of(mt, s)
        return remote(part, part, gx_send.at[to, s], gx_recv.at[chip, s], {"tp": to * 2 + core})

    def to_mate(step, s):
        origin = lax.rem(chip + step, chips)
        part = chunk_of(origin * 2 + core, s)
        return remote(part, part, gc_send.at[origin, s], gc_recv.at[origin, s], {"tp": mate})

    def expert_rows(e):
        return pl.ds(pl.multiple_of(e * cap_e, cap_e), cap_e)

    def h_over_x(step, e):
        to = lax.rem(chip + step, chips)
        return remote(
            hmine.at[expert_rows(e)], hall.at[mt, expert_rows(e)],
            hx_send.at[to, e], hx_recv.at[chip, e], {"tp": to * 2 + core},
        )

    def h_to_mate(step, e):
        origin = lax.rem(chip + step, chips)
        part = hall.at[origin * 2 + core, expert_rows(e)]
        src = hmine.at[expert_rows(e)] if step == 0 else part
        return remote(src, part, hc_send.at[origin, e], hc_recv.at[origin, e], {"tp": mate})

    def h_relay(e):
        for step in range(1, chips):
            origin = lax.rem(chip + step, chips)
            landed(hall.at[origin * 2 + core, expert_rows(e)], hx_recv.at[origin, e])
            h_to_mate(step, e).start()

    def giving(step, part):
        to = lax.rem(me + step, ep)
        lanes = slice(part * wide_part, (part + 1) * wide_part)
        return remote(
            ret_out.at[pl.ds(pl.multiple_of(to * cap, cap), cap), lanes],
            ret_in.at[pl.ds(pl.multiple_of(me * cap, cap), cap), lanes],
            r_send.at[to, part], r_recv.at[me, part], {"ep": to},
        )

    def landed(dst, sem):
        pltpu.make_async_copy(dst, dst, sem).wait()

    pl.semaphore_wait(barrier, ep - 1 + tp - 1)
    for step in range(1, ep):
        dispatch(step).start()
        tell(step).start()
    for step in range(1, tp):
        gains(step).start()

    def forward(j):
        s = lax.rem(me + j, ep)
        if j > 0:
            landed(chunk_of(mt, s), d_recv.at[s])
        for step in range(1, chips):
            over_x(step, s).start()
        to_mate(0, s).start()

    def relay(j):
        s = lax.rem(me + j, ep)
        for step in range(1, chips):
            origin = lax.rem(chip + step, chips)
            landed(chunk_of(origin * 2 + core, s), gx_recv.at[origin, s])
            to_mate(step, s).start()

    order = [j for near in range(1, ep // 2 + 1) for j in sorted({near, ep - near})]
    forward(0)

    for src, dst in ((k_ref, k_s), (v_ref, v_s), (q_ref, q_s)):
        rows_s[...] = src[...].astype(F32)
        for h in range(heads):
            for c in range(length // 128):
                dst[c * 128 : (c + 1) * 128, h * 128 : (h + 1) * 128] = rows_s[
                    pl.ds(c * 128 * heads + h, 128, stride=heads), :
                ].astype(BF16)

    strengths = 1.0 / (1.0 + jnp.exp(-beta_ref[...]))
    for h in range(heads):
        beta_s[h] = strengths[h : h + 1]
    raw = decay_ref[...]
    small = jnp.exp(-jnp.abs(raw))
    bigger = 1.0 + small
    diff = bigger - 1.0
    log_term = jnp.where(
        diff == 0.0, small, jnp.log(bigger) * small / jnp.where(diff == 0.0, 1.0, diff)
    )
    rates = jnp.maximum(raw, 0.0) + log_term
    ones_upper = (iota((128, 128), 0) <= iota((128, 128), 1)).astype(F32)
    for c in range(length // 128):
        here = slice(c * 128, (c + 1) * 128)
        summed = -exact(rates[:, here], ones_upper)
        for h in range(heads):
            cum_s[h, :, here] = summed[h : h + 1]

    def chain_copy(h):
        return remote(sout_s.at[h], sin_s.at[h], c_send.at[h], c_recv.at[h], {"ep": lax.rem(me + 1, ep)})

    def one_head(h, carry):
        def service():
            @pl.when(h == 1)
            def _():
                relay(0)

            @pl.when(h == 2)
            def _():
                for j in order[:-1]:
                    relay(j)

        state_part(h, k_s, v_s, cum_s, beta_s, wu_s, z_s, m_s, n_s, service)

        @pl.when(me == 0)
        def _():
            sout_s[h] = n_s[h]
            chain_copy(h).start()

        @pl.when(h == 0)
        def _():
            for j in order[:-1]:
                forward(j)

        @pl.when(h == 1)
        def _():
            forward(order[-1])

        @pl.when(h == 2)
        def _():
            relay(order[-1])

        return carry

    lax.fori_loop(0, heads, one_head, 0)

    def chain_turn(low, high):
        def turn(h, carry):
            landed(sin_s.at[h], c_recv.at[h])

            @pl.when(me < ep - 1)
            def _():
                sout_s[h] = dot3(m_s[h], sin_s[h]) + n_s[h]
                chain_copy(h).start()

            return carry

        def all_turns():
            lax.fori_loop(low, high, turn, 0)

        return all_turns

    def outputs(low, high):
        def one(h, carry):
            output_part(h, q_s, k_s, cum_s, wu_s, z_s, gp_s, y_s)
            return carry

        lax.fori_loop(low, high, one, 0)

    last = heads - 1
    pl.when(me == 1)(chain_turn(0, last))

    for step in range(1, ep):
        s = lax.rem(me + step, ep)
        landed(info_all.at[s], i_recv.at[s])
    r_in, r_out = iota((tokens, tokens), 0), iota((tokens, tokens), 1)
    told = jnp.zeros((n_rows, tokens), F32)
    for s in range(ep):
        take = (r_in - me * cap == r_out - s * cap) & (r_out >= s * cap) & (r_out < (s + 1) * cap)
        told = told + exact(info_all[s], take.astype(F32))
    ranks = mm(told.astype(BF16), upper)
    for e in range(local):
        where_to = iota((cap_e, tokens), 0).astype(F32) == ranks[e : e + 1]
        placed = jnp.where(where_to, told[e : e + 1], 0.0)
        place_s[e * cap_e : (e + 1) * cap_e, :] = placed.astype(BF16)
        left = jnp.transpose(placed * told[local + e : local + e + 1])
        for piece in range(back_s.shape[0]):
            taken = left.astype(BF16)
            back_s[piece, :, e * cap_e : (e + 1) * cap_e] = taken
            left = left - taken.astype(F32)

    for step in range(1, tp):
        t = lax.rem(mt + step, tp)
        landed(gall.at[t], g_recv.at[t])
    for step in range(chips):
        origin = lax.rem(chip + step, chips)
        for s in range(ep):
            landed(chunk_of(origin * 2 + 1 - core, s), gc_recv.at[origin, s])

    def squares(t, total):
        part = xall[t].astype(F32)
        return total + jnp.sum(part * part, -1, keepdims=True)

    total = lax.fori_loop(0, tp, squares, jnp.zeros((tokens, 1), F32))
    scale = lax.rsqrt(total / (tp * dl) + EPSILON)

    def spread_rows(t, carry):
        normed = (xall[t].astype(F32) * scale * gall[t]).astype(BF16)
        xe[:, pl.ds(pl.multiple_of(t * dl, dl), dl)] = mm(place_s[...], normed).astype(BF16)
        return carry

    lax.fori_loop(0, tp, spread_rows, 0)

    def one_expert(e, carry):
        rows = pl.ds(pl.multiple_of(e * cap_e, cap_e), cap_e)
        weight(0, e).wait()
        weight(1, e).wait()
        gate = mm(xe[rows, :], wg_v[e])
        up = mm(xe[rows, :], wu_v[e])
        hidden = (gate / (1.0 + jnp.exp(-gate)) * up).astype(BF16)
        hmine[rows, :] = hidden
        hall[mt, rows, :] = hidden
        for step in range(1, chips):
            h_over_x(step, e).start()
        h_to_mate(0, e).start()
        return carry

    lax.fori_loop(0, local, one_expert, 0)
    h_relay(0)
    pl.when(me == 1)(chain_turn(last, heads))
    pl.when(me == 2)(chain_turn(0, last))
    outputs(0, 1)
    for e in range(1, local):
        h_relay(e)
    outputs(1, 2)
    pl.when(me == 2)(chain_turn(last, heads))
    pl.when(me >= 3)(chain_turn(0, last))
    for e in range(local):
        for step in range(chips):
            origin = lax.rem(chip + step, chips)
            landed(hall.at[origin * 2 + 1 - core, expert_rows(e)], hc_recv.at[origin, e])

    for e in range(local):
        weight(2, e).wait()
    own = pl.ds(pl.multiple_of(me * cap, cap), cap)
    for t in range(tp):
        wide_s[:, t * hall.shape[2] : (t + 1) * hall.shape[2]] = hall[t]
    for part in range(parts):
        lanes = slice(part * wide_part, (part + 1) * wide_part)
        for e in range(local):
            rows = slice(e * cap_e, (e + 1) * cap_e)
            copies_s[rows, lanes] = mm(wide_s[rows, :], wd_v[e, :, lanes]).astype(BF16)
        result = mm(back_s[0], copies_s[:, lanes])
        for piece in range(1, back_s.shape[0]):
            result = result + mm(back_s[piece], copies_s[:, lanes])
        ret_out[:, lanes] = result.astype(BF16)
        ret_in[own, lanes] = ret_out[own, lanes]
        for step in range(1, ep):
            giving(step, part).start()

    outputs(2, heads)
    pl.when(me >= 3)(chain_turn(last, heads))

    @pl.when(me == 0)
    def _():
        sin_s[...] = jnp.zeros_like(sin_s)

    for h in range(heads):
        mixed = dot3(gp_s[h], sin_s[h]) + y_s[h]
        normed = mixed * lax.rsqrt(jnp.mean(mixed * mixed, -1, keepdims=True) + EPSILON)
        rows_s[pl.ds(h, length, stride=heads), :] = normed * ngain_ref[...]
    mix_ref[...] = rows_s[...].astype(BF16)

    for step in range(1, ep):
        s = lax.rem(me + step, ep)
        for part in range(parts):
            lanes = slice(part * wide_part, (part + 1) * wide_part)
            landed(ret_in.at[pl.ds(pl.multiple_of(s * cap, cap), cap), lanes], r_recv.at[s, part])
    ffn_ref[...] = mm(perm_s[...], ret_in[...], COLS_COLS).astype(BF16)

    for step in range(1, ep):
        dispatch(step).wait_send()
        tell(step).wait_send()
        for part in range(parts):
            giving(step, part).wait_send()
    for step in range(1, tp):
        gains(step).wait_send()
    for step in range(1, chips):
        for e in range(local):
            h_over_x(step, e).wait_send()
        for s in range(ep):
            over_x(step, s).wait_send()
    for step in range(chips):
        for e in range(local):
            h_to_mate(step, e).wait_send()
        for s in range(ep):
            to_mate(step, s).wait_send()

    @pl.when(me < ep - 1)
    def _():
        def sent(h, carry):
            chain_copy(h).wait_send()
            return carry

        lax.fori_loop(0, heads, sent, 0)


def hand_on(mix_ref, ffn_ref, mix_out, ffn_out):
    mix_out[...] = mix_ref[...]
    ffn_out[...] = ffn_ref[...]


def fused_body(
    mix_query, mix_keys, mix_values, beta_in, decay_in, norm_gain, ffn_input, ffn_gain,
    expert_ids, expert_share, w_gate, w_up, w_down,
):
    ep, tp = lax.axis_size("ep"), lax.axis_size("tp")
    length, heads, width = mix_query.shape
    tokens, dl = ffn_input.shape
    local, full, fl = w_gate.shape
    out_width = w_down.shape[2]
    picks = expert_ids.shape[1]
    n_rows = max(8, 2 * local)
    chips = tp // 2
    rows_e = tokens * picks
    parts = max(1, min(2, out_width // 512))
    dma = pltpu.SemaphoreType.DMA
    vmem = pl.BlockSpec(memory_space=pltpu.VMEM)
    hbm = pl.BlockSpec(memory_space=pl.ANY)
    state = pltpu.VMEM((heads, width, width), F32)
    wide_state = pltpu.VMEM((heads, length, width), F32)
    mix_out, ffn_out = pl.pallas_call(
        layer_kernel,
        out_shape=(
            jax.ShapeDtypeStruct((length * heads, width), BF16),
            jax.ShapeDtypeStruct((tokens, out_width), BF16),
        ),
        in_specs=[vmem] * 10 + [hbm] * 3,
        out_specs=(vmem, vmem),
        scratch_shapes=[
            pltpu.VMEM((length, heads * width), BF16),
            pltpu.VMEM((length, heads * width), BF16),
            pltpu.VMEM((length, heads * width), BF16),
            pltpu.VMEM((length * heads, width), F32),
            pltpu.VMEM((heads, length, 2 * width), F32),
            pltpu.VMEM((heads, max(length // 128 - 1, 1), width, 2 * width), F32),
            pltpu.VMEM((heads, 1, length), F32),
            pltpu.VMEM((heads, 1, length), F32),
            wide_state,
            wide_state,
            state,
            state,
            state,
            state,
            pltpu.VMEM(w_gate.shape, BF16),
            pltpu.VMEM(w_up.shape, BF16),
            pltpu.VMEM(w_down.shape, BF16),
            pltpu.VMEM((tokens, tokens), BF16),
            pltpu.VMEM((tokens, dl), BF16),
            pltpu.VMEM((n_rows, tokens), F32),
            pltpu.VMEM((ep, n_rows, tokens), F32),
            pltpu.VMEM((tp, 1, dl), F32),
            pltpu.VMEM((tp, tokens, dl), BF16),
            pltpu.VMEM((rows_e, full), BF16),
            pltpu.VMEM((rows_e, fl), BF16),
            pltpu.VMEM((tp, rows_e, fl), BF16),
            pltpu.VMEM((rows_e, tokens), BF16),
            pltpu.VMEM((3, tokens, rows_e), BF16),
            pltpu.VMEM((rows_e, tp * fl), BF16),
            pltpu.VMEM((rows_e, out_width), BF16),
            pltpu.VMEM((tokens, out_width), BF16),
            pltpu.VMEM((tokens, out_width), BF16),
            dma((3, local)),
            dma((ep,)), dma((ep,)), dma((ep,)), dma((ep,)),
            dma((tp,)), dma((tp,)),
            dma((chips, ep)), dma((chips, ep)), dma((chips, ep)), dma((chips, ep)),
            dma((chips, local)), dma((chips, local)), dma((chips, local)), dma((chips, local)),
            dma((ep, parts)), dma((ep, parts)),
            dma((heads,)), dma((heads,)),
        ],
        compiler_params=pltpu.CompilerParams(
            collective_id=0, has_side_effects=True, vmem_limit_bytes=60 * 1024 * 1024
        ),
    )(
        mix_query.reshape(length * heads, width),
        mix_keys.reshape(length * heads, width),
        mix_values.reshape(length * heads, width),
        beta_in, decay_in, norm_gain.reshape(1, width),
        ffn_input, ffn_gain.reshape(1, dl), expert_ids.T, expert_share.T,
        w_gate, w_up, w_down,
    )
    mix_out, ffn_out = pl.pallas_call(
        hand_on,
        out_shape=(
            jax.ShapeDtypeStruct(mix_out.shape, BF16),
            jax.ShapeDtypeStruct(ffn_out.shape, BF16),
        ),
        in_specs=[vmem] * 2,
        out_specs=(vmem, vmem),
        cost_estimate=pl.CostEstimate(flops=1000, bytes_accessed=2**21, transcendentals=0),
    )(mix_out, ffn_out)
    return (mix_out.reshape(length, heads, width), ffn_out)


def body(
    mix_query,
    mix_keys,
    mix_values,
    beta_in,
    decay_in,
    norm_gain,
    ffn_input,
    ffn_gain,
    expert_ids,
    expert_share,
    w_gate,
    w_up,
    w_down,
):
    width, local = mix_query.shape[2], w_gate.shape[0]
    whole_groups = local % GROUP == 0 and expert_ids.shape[1] == 2
    even = lax.axis_size("tp") % 2 == 0 and lax.axis_size("tp") > 1 and lax.axis_size("ep") > 1
    if whole_groups and even and mix_query.shape[1] > 3 and width == 128 and mix_query.shape[0] % 128 == 0:
        return fused_body(
            mix_query,
            mix_keys,
            mix_values,
            beta_in,
            decay_in,
            norm_gain,
            ffn_input,
            ffn_gain,
            expert_ids,
            expert_share,
            w_gate,
            w_up,
            w_down,
        )
    mix_out = mixer_body(mix_query, mix_keys, mix_values, beta_in, decay_in, norm_gain)
    ffn_out = experts_body(ffn_input, ffn_gain, expert_ids, expert_share, w_gate, w_up, w_down)
    return (mix_out, ffn_out)


def solution(mesh):
    placed = (
        P(("grp", "ep"), "tp", None),
        P(("grp", "ep"), "tp", None),
        P(("grp", "ep"), "tp", None),
        P("tp", ("grp", "ep")),
        P("tp", ("grp", "ep")),
        P(),
        P(("grp", "ep"), "tp"),
        P("tp"),
        P(("grp", "ep"), None),
        P(("grp", "ep"), None),
        P("ep", None, "tp"),
        P("ep", None, "tp"),
        P("ep", None, "tp"),
    )
    return jax.shard_map(
        body,
        mesh=mesh,
        in_specs=placed,
        out_specs=(P(("grp", "ep"), "tp", None), P(("grp", "ep"), "tp")),
        check_vma=False,
    )
```

profile of v0, /device:TPU:0, one launch (start us, length us, event | category | flops | bytes accessed | tf_op | source)
XLA Modules:
  0.0 46.6 jit_solution(9041118651514859442)
XLA Ops:
  0.6 43.9 %shard_map.140 = (bf16[2048,128]{1,0:T(8,128)(2,1)}, bf16[128,1024]{1,0:T(8,128)(2,1)}) custom-call(bf16[2048,128]{1,0:T(8,128)(2,1)} %bitcast.8, bf16[2048,128]{1,0:T(8,128)(2,1)} %bitcast.9, bf16[2048,128]{1,0:T(8,128)(2,1)} %bitcast.10, f32[4,512]{1,0:T(4,128)} %beta_ref.1, f32[4,512]{1,0:T(4,128)} %decay_ref.1, f32[1,128]{1,0:T(1,128)} %bitcast.14, ...), custom_call_target="tpu_custom_call" | custom-call | tf_op jit(solution)/shard_map/pallas_call | solution.py:703
  44.6 2.0 %shard_map.141 = (bf16[2048,128]{1,0:T(8,128)(2,1)}, bf16[128,1024]{1,0:T(8,128)(2,1)}) custom-call(bf16[2048,128]{1,0:T(8,128)(2,1)} %get-tuple-element.6.mix_ref, bf16[128,1024]{1,0:T(8,128)(2,1)} %get-tuple-element.7.ffn_ref), custom_call_target="tpu_custom_call" | custom-call | flops 1000 | bytes 2097152 | tf_op jit(solution)/shard_map/pallas_call | solution.py:763
where the time goes:
time: 46.8 us; the launch traced here: 46.6 us
  Pallas kernels  45.9 us (98%)
  between operations  0.64 us (1%)
    pallas_call x1, Pallas kernels, fused_body(): pl.pallas_call(layer_kernel, out_shape=(jax.ShapeDtypeStruct((length * he...  43.9 us
    pallas_call x1, Pallas kernels, fused_body(): pl.pallas_call(hand_on, out_shape=(jax.ShapeDtypeStruct(mix_out.shape, BF...  2.02 us

commit v1 on v0

--- a/solution.py
+++ b/solution.py
@@ -177,121 +177,143 @@
     return high, (a - high.astype(F32)).astype(BF16)
 
 
-def dot3(a, b):
-    ah, al = halves(a)
+def joined(parts, dim):
+    return jnp.concatenate(parts, dim)
+
+
+def split(a):
+    return joined(halves(a), 1)
+
+
+def twice(b):
+    return joined([b, b], 0)
+
+
+def three(a, b):
+    n = b.shape[1]
     bh, bl = halves(b)
-    return mm(ah, bh) + mm(ah, bl) + mm(al, bh)
+    rhs = joined([joined([bh, bl], 1), joined([bh, jnp.zeros_like(bl)], 1)], 0)
+    out = mm(split(a), rhs)
+    return out[:, :n] + out[:, n:]
 
 
 def iota(shape, dim):
     return lax.broadcasted_iota(jnp.int32, shape, dim)
 
 
-def flipped(row, n):
-    return jnp.transpose(jnp.broadcast_to(row, (n, n)))
-
-
-def decays(h, here, k, cum_s):
-    n = k.shape[0]
-    kf = k.astype(F32)
-    rk = lax.rsqrt(jnp.sum(kf * kf, -1, keepdims=True) + EPSILON)
-    rk_t = jnp.transpose(jnp.broadcast_to(rk, (n, n)))
-    crow = cum_s[h, :, here]
-    ccol = flipped(crow, n)
-    causal = iota((n, n), 0) >= iota((n, n), 1)
-    dm = jnp.where(causal, jnp.exp(jnp.where(causal, ccol - crow, 0.0)), 0.0) * rk_t
-    return rk, rk_t, crow, ccol, dm
-
-
-def state_part(h, k_ref, v_ref, cum_s, beta_s, wu_s, z_s, m_s, n_s, service):
+def pair_rows(h, c, chunks):
+    return (h % 2) * chunks + c
+
+
+def state_pair(g, q_ref, k_ref, v_ref, rows_s, cols_s, gp_s, sc_s, wu_s, z_s, m_s, n_s, service):
     length = k_ref.shape[0]
     n = 128
-    chunks = range(length // n)
-    lanes = pl.ds(pl.multiple_of(h * n, n), n)
+    chunks = length // n
+    count = 2 * chunks
+    units = [(i, c) for i in range(2) for c in range(chunks)]
     row, col = iota((n, n), 0), iota((n, n), 1)
-    strict = row > col
+    causal, strict = row >= col, row > col
     same = (row >= n // 2) == (col >= n // 2)
     eye = (row == col).astype(F32)
+
+    def block(ref, u):
+        i, c = units[u]
+        return ref[c * n : (c + 1) * n, pl.ds(pl.multiple_of((2 * g + i) * n, n), n)]
+
+    def row_of(kind, u):
+        return rows_s[g, kind * count + u : kind * count + u + 1, :]
+
+    def col_of(kind, u):
+        return cols_s[g, :, kind * count + u : kind * count + u + 1]
+
+    everything = range(count)
+    rks, gathered = [], jnp.zeros((n, n), F32)
+    for u in everything:
+        kf = block(k_ref, u).astype(F32)
+        rk = lax.rsqrt(jnp.sum(kf * kf, -1, keepdims=True) + EPSILON)
+        rks.append(rk)
+        gathered = jnp.where(col == u, rk, gathered)
+    rows_s[g, 2 * count : 3 * count, :] = jnp.transpose(gathered)[:count]
     prods, powers, offs, tails, rowsets = [], [], [], [], []
-    for c in chunks:
-        here = slice(c * n, (c + 1) * n)
-        k = k_ref[here, lanes]
-        rk, rk_t, crow, ccol, dm = decays(h, here, k, cum_s)
-        brow = beta_s[h, :, here]
-        bcol = flipped(brow, n)
-        lower = jnp.where(strict, mm(k, k, ROWS_ROWS) * dm * (rk * bcol), 0.0)
+    for u in everything:
+        i, c = units[u]
+        k, q = block(k_ref, u), block(q_ref, u)
+        qf = q.astype(F32)
+        rq = lax.rsqrt(jnp.sum(qf * qf, -1, keepdims=True) + EPSILON) * (n ** (-0.5))
+        crow, brow, rkrow = row_of(0, u), row_of(1, u), row_of(2, u)
+        ccol, bcol = col_of(0, u), col_of(1, u)
+        raw = mm(joined([k, q], 0), k, ROWS_ROWS)
+        dm = jnp.where(causal, jnp.exp(jnp.where(causal, ccol - crow, 0.0)), 0.0) * rkrow
+        lower = jnp.where(strict, raw[:n] * dm * (rks[u] * bcol), 0.0)
+        sc_s[g, u] = split(raw[n:] * dm * rq)
+        gp_s[g, u] = qf * (rq * jnp.exp(ccol))
         neg = jnp.where(same, -lower, 0.0)
         offs.append(jnp.where(same, 0.0, lower))
         prods.append(eye + neg)
         powers.append(neg)
         clast = crow[:, n - 1 :]
-        tails.append((rk * jnp.exp(clast - ccol), jnp.exp(clast)))
-        rowsets.append((brow, brow * rk_t * jnp.exp(crow)))
-    powers = [dot3(p, p) for p in powers]
+        tails.append((rks[u] * jnp.exp(clast - ccol), jnp.exp(clast)))
+        rowsets.append((brow, brow * rkrow * jnp.exp(crow)))
+    powers = [three(p, p) for p in powers]
+    service(0)
     for turn in range((BLOCK - 1).bit_length() - 2):
-        both = [dot3(jnp.concatenate([a, p], 0), p) for a, p in zip(prods, powers)]
+        both = [three(joined([a, p], 0), p) for a, p in zip(prods, powers)]
         prods = [a + b[:n] for a, b in zip(prods, both)]
         powers = [b[n:] for b in both]
-        if turn == 1:
-            service()
-    prods = [a + dot3(a, p) for a, p in zip(prods, powers)]
-    mids = [dot3(o, a) for o, a in zip(offs, prods)]
-    prods = [a - dot3(a, m) for a, m in zip(prods, mids)]
+    service(1)
+    prods = [a + three(a, p) for a, p in zip(prods, powers)]
+    mids = [three(o, a) for o, a in zip(offs, prods)]
+    prods = [a - three(a, m) for a, m in zip(prods, mids)]
     pairs = []
-    for c in chunks:
+    for u in everything:
+        k, v = block(k_ref, u), block(v_ref, u)
+        x, w = prods[u] * rowsets[u][0], prods[u] * rowsets[u][1]
+        pairs.append(joined([mm(split(w), twice(k)), mm(split(x), twice(v))], 1))
+        wu_s[g, u] = pairs[u].astype(BF16)
+    service(2)
+    steps = []
+    for u in everything:
+        scale, last = tails[u]
+        sh, sl = halves(pairs[u] * scale)
+        k = block(k_ref, u)
+        moved = mm(twice(k), joined([sh, sl], 0), COLS_COLS)
+        steps.append((last * eye - moved[:, :n], moved[:, n:]))
+    states = [None, None]
+    for c in range(chunks):
+        for i in range(2):
+            step, add = steps[i * chunks + c]
+            if c == 0:
+                states[i] = joined([step, add], 1)
+            else:
+                z_s[g, i * (chunks - 1) + c - 1] = states[i].astype(BF16)
+                sh, sl = halves(states[i])
+                th, tl = halves(step)
+                out = mm(joined([th, tl], 1), twice(sh)) + mm(th, sl)
+                states[i] = out + joined([jnp.zeros_like(add), add], 1)
+    for i in range(2):
+        m_s[2 * g + i] = split(states[i][:, :n])
+        n_s[2 * g + i] = states[i][:, n:]
+
+
+def output_pair(g, gp_s, sc_s, wu_s, z_s, gs_s, y_s, chunks):
+    n = 128
+    count = 2 * chunks
+    spreads = [mm(sc_s[g, u], twice(wu_s[g, u])) for u in range(count)]
+    for u in range(count):
+        i, c = u // chunks, u % chunks
+        reader, base = gp_s[g, u] - spreads[u][:, :n], spreads[u][:, n:]
+        if c > 0:
+            both = mm(split(reader), twice(z_s[g, i * (chunks - 1) + c - 1]))
+            reader, base = both[:, :n], both[:, n:] + base
         here = slice(c * n, (c + 1) * n)
-        uh, ul = halves(prods[c] * rowsets[c][0])
-        wh, wl = halves(prods[c] * rowsets[c][1])
-        k, v = k_ref[here, lanes], v_ref[here, lanes]
-        pairs.append(jnp.concatenate([mm(wh, k) + mm(wl, k), mm(uh, v) + mm(ul, v)], 1))
-        wu_s[h, here, :] = pairs[c]
-    state = None
-    for c in chunks:
-        here = slice(c * n, (c + 1) * n)
-        scale, last = tails[c]
-        sh, sl = halves(pairs[c] * jnp.concatenate([scale, scale], 1))
-        k = k_ref[here, lanes]
-        moved = mm(k, sh, COLS_COLS) + mm(k, sl, COLS_COLS)
-        step, add = last * eye - moved[:, :n], moved[:, n:]
-        if state is None:
-            state = jnp.concatenate([step, add], 1)
-        else:
-            z_s[h, c - 1] = state
-            state = dot3(step, state) + jnp.concatenate([jnp.zeros_like(add), add], 1)
-    m_s[h] = state[:, :n]
-    n_s[h] = state[:, n:]
-
-
-def output_part(h, q_ref, k_ref, cum_s, wu_s, z_s, gp_s, y_s):
-    length = q_ref.shape[0]
-    n = 128
-    lanes = pl.ds(pl.multiple_of(h * n, n), n)
-    chunks = range(length // n)
-    spreads, qds = [], []
-    for c in chunks:
-        here = slice(c * n, (c + 1) * n)
-        q, k = q_ref[here, lanes], k_ref[here, lanes]
-        qf = q.astype(F32)
-        rq = lax.rsqrt(jnp.sum(qf * qf, -1, keepdims=True) + EPSILON) * (n ** (-0.5))
-        _, _, _, ccol, dm = decays(h, here, k, cum_s)
-        spreads.append(dot3(mm(q, k, ROWS_ROWS) * dm * rq, wu_s[h, here, :]))
-        qds.append(qf * rq * jnp.exp(ccol))
-    for c in chunks:
-        here = slice(c * n, (c + 1) * n)
-        reader, base = qds[c] - spreads[c][:, :n], spreads[c][:, n:]
-        if c == 0:
-            gp_s[h, here, :] = reader
-            y_s[h, here, :] = base
-        else:
-            both = dot3(reader, z_s[h, c - 1])
-            gp_s[h, here, :] = both[:, :n]
-            y_s[h, here, :] = both[:, n:] + base
+        gs_s[2 * g + i, here, :] = split(reader)
+        y_s[2 * g + i, here, :] = base
 
 
 def layer_kernel(
     q_ref, k_ref, v_ref, beta_ref, decay_ref, ngain_ref, x_ref, gain_ref, ids_ref, share_ref,
     wg_ref, wu_ref, wd_ref, mix_ref, ffn_ref,
-    q_s, k_s, v_s, rows_s, wu_s, z_s, cum_s, beta_s, gp_s, y_s, m_s, n_s, sin_s, sout_s,
+    q_s, k_s, v_s, flat_s, rows_s, cols_s, sc_s, wu_s, z_s, gp_s, gs_s, y_s, m_s, n_s, sin_s, sout_s,
     wg_v, wu_v, wd_v, perm_s, disp, info_out, info_all, gall, xall, xe, hmine, hall, place_s, back_s, wide_s, copies_s,
     ret_out, ret_in,
     w_sem, d_send, d_recv, i_send, i_recv, g_send, g_recv,
@@ -452,16 +474,14 @@
     forward(0)
 
     for src, dst in ((k_ref, k_s), (v_ref, v_s), (q_ref, q_s)):
-        rows_s[...] = src[...].astype(F32)
+        flat_s[...] = src[...].astype(F32)
         for h in range(heads):
             for c in range(length // 128):
-                dst[c * 128 : (c + 1) * 128, h * 128 : (h + 1) * 128] = rows_s[
+                dst[c * 128 : (c + 1) * 128, h * 128 : (h + 1) * 128] = flat_s[
                     pl.ds(c * 128 * heads + h, 128, stride=heads), :
                 ].astype(BF16)
 
     strengths = 1.0 / (1.0 + jnp.exp(-beta_ref[...]))
-    for h in range(heads):
-        beta_s[h] = strengths[h : h + 1]
     raw = decay_ref[...]
     small = jnp.exp(-jnp.abs(raw))
     bigger = 1.0 + small
@@ -471,49 +491,51 @@
     )
     rates = jnp.maximum(raw, 0.0) + log_term
     ones_upper = (iota((128, 128), 0) <= iota((128, 128), 1)).astype(F32)
-    for c in range(length // 128):
+    chunks = length // 128
+    rows_s[...] = jnp.zeros_like(rows_s)
+    for c in range(chunks):
         here = slice(c * 128, (c + 1) * 128)
         summed = -exact(rates[:, here], ones_upper)
         for h in range(heads):
-            cum_s[h, :, here] = summed[h : h + 1]
+            u = pair_rows(h, c, chunks)
+            rows_s[h // 2, u : u + 1, :] = summed[h : h + 1]
+            rows_s[h // 2, 2 * chunks + u : 2 * chunks + u + 1, :] = strengths[h : h + 1, here]
+    for g in range(heads // 2):
+        cols_s[g] = jnp.transpose(rows_s[g])
 
     def chain_copy(h):
         return remote(sout_s.at[h], sin_s.at[h], c_send.at[h], c_recv.at[h], {"ep": lax.rem(me + 1, ep)})
 
-    def one_head(h, carry):
-        def service():
-            @pl.when(h == 1)
-            def _():
-                relay(0)
-
-            @pl.when(h == 2)
-            def _():
-                for j in order[:-1]:
-                    relay(j)
-
-        state_part(h, k_s, v_s, cum_s, beta_s, wu_s, z_s, m_s, n_s, service)
+    def one_pair(g, carry):
+        def service(place):
+            if place == 1:
+                @pl.when(g == 0)
+                def _():
+                    for j in order[:-1]:
+                        forward(j)
+
+                @pl.when(g == 1)
+                def _():
+                    for j in order[:-1]:
+                        relay(j)
+
+        state_pair(g, q_s, k_s, v_s, rows_s, cols_s, gp_s, sc_s, wu_s, z_s, m_s, n_s, service)
 
         @pl.when(me == 0)
         def _():
-            sout_s[h] = n_s[h]
-            chain_copy(h).start()
-
-        @pl.when(h == 0)
+            for i in range(2):
+                sout_s[2 * g + i] = n_s[2 * g + i].astype(BF16)
+                chain_copy(2 * g + i).start()
+
+        @pl.when(g == 0)
         def _():
-            for j in order[:-1]:
-                forward(j)
-
-        @pl.when(h == 1)
-        def _():
+            relay(0)
             forward(order[-1])
 
-        @pl.when(h == 2)
-        def _():
-            relay(order[-1])
-
         return carry
 
-    lax.fori_loop(0, heads, one_head, 0)
+    lax.fori_loop(0, heads // 2, one_pair, 0)
+    relay(order[-1])
 
     def chain_turn(low, high):
         def turn(h, carry):
@@ -521,7 +543,7 @@
 
             @pl.when(me < ep - 1)
             def _():
-                sout_s[h] = dot3(m_s[h], sin_s[h]) + n_s[h]
+                sout_s[h] = (mm(m_s[h], twice(sin_s[h])) + n_s[h]).astype(BF16)
                 chain_copy(h).start()
 
             return carry
@@ -533,7 +555,7 @@
 
     def outputs(low, high):
         def one(h, carry):
-            output_part(h, q_s, k_s, cum_s, wu_s, z_s, gp_s, y_s)
+            output_pair(h, gp_s, sc_s, wu_s, z_s, gs_s, y_s, chunks)
             return carry
 
         lax.fori_loop(low, high, one, 0)
@@ -603,7 +625,6 @@
     outputs(0, 1)
     for e in range(1, local):
         h_relay(e)
-    outputs(1, 2)
     pl.when(me == 2)(chain_turn(last, heads))
     pl.when(me >= 3)(chain_turn(0, last))
     for e in range(local):
@@ -629,7 +650,7 @@
         for step in range(1, ep):
             giving(step, part).start()
 
-    outputs(2, heads)
+    outputs(1, heads // 2)
     pl.when(me >= 3)(chain_turn(last, heads))
 
     @pl.when(me == 0)
@@ -637,10 +658,10 @@
         sin_s[...] = jnp.zeros_like(sin_s)
 
     for h in range(heads):
-        mixed = dot3(gp_s[h], sin_s[h]) + y_s[h]
+        mixed = mm(gs_s[h], twice(sin_s[h])) + y_s[h]
         normed = mixed * lax.rsqrt(jnp.mean(mixed * mixed, -1, keepdims=True) + EPSILON)
-        rows_s[pl.ds(h, length, stride=heads), :] = normed * ngain_ref[...]
-    mix_ref[...] = rows_s[...].astype(BF16)
+        flat_s[pl.ds(h, length, stride=heads), :] = normed * ngain_ref[...]
+    mix_ref[...] = flat_s[...].astype(BF16)
 
     for step in range(1, ep):
         s = lax.rem(me + step, ep)
@@ -698,8 +719,7 @@
     dma = pltpu.SemaphoreType.DMA
     vmem = pl.BlockSpec(memory_space=pltpu.VMEM)
     hbm = pl.BlockSpec(memory_space=pl.ANY)
-    state = pltpu.VMEM((heads, width, width), F32)
-    wide_state = pltpu.VMEM((heads, length, width), F32)
+    pairs, chunks = heads // 2, length // width
     mix_out, ffn_out = pl.pallas_call(
         layer_kernel,
         out_shape=(
@@ -713,16 +733,18 @@
             pltpu.VMEM((length, heads * width), BF16),
             pltpu.VMEM((length, heads * width), BF16),
             pltpu.VMEM((length * heads, width), F32),
-            pltpu.VMEM((heads, length, 2 * width), F32),
-            pltpu.VMEM((heads, max(length // 128 - 1, 1), width, 2 * width), F32),
-            pltpu.VMEM((heads, 1, length), F32),
-            pltpu.VMEM((heads, 1, length), F32),
-            wide_state,
-            wide_state,
-            state,
-            state,
-            state,
-            state,
+            pltpu.VMEM((pairs, 128, 128), F32),
+            pltpu.VMEM((pairs, 128, 128), F32),
+            pltpu.VMEM((pairs, 2 * chunks, width, 2 * width), BF16),
+            pltpu.VMEM((pairs, 2 * chunks, width, 2 * width), BF16),
+            pltpu.VMEM((pairs, max(2 * (chunks - 1), 1), width, 2 * width), BF16),
+            pltpu.VMEM((pairs, 2 * chunks, width, width), F32),
+            pltpu.VMEM((heads, length, 2 * width), BF16),
+            pltpu.VMEM((heads, length, width), F32),
+            pltpu.VMEM((heads, width, 2 * width), BF16),
+            pltpu.VMEM((heads, width, width), F32),
+            pltpu.VMEM((heads, width, width), BF16),
+            pltpu.VMEM((heads, width, width), BF16),
             pltpu.VMEM(w_gate.shape, BF16),
             pltpu.VMEM(w_up.shape, BF16),
             pltpu.VMEM(w_down.shape, BF16),
@@ -791,7 +813,7 @@
     width, local = mix_query.shape[2], w_gate.shape[0]
     whole_groups = local % GROUP == 0 and expert_ids.shape[1] == 2
     even = lax.axis_size("tp") % 2 == 0 and lax.axis_size("tp") > 1 and lax.axis_size("ep") > 1
-    if whole_groups and even and mix_query.shape[1] > 3 and width == 128 and mix_query.shape[0] % 128 == 0:
+    if whole_groups and even and mix_query.shape[1] == 4 and width == 128 and mix_query.shape[0] % 128 == 0:
         return fused_body(
             mix_query,
             mix_keys,

time: 46.8 us -> 43.6 us (0.932)
  Pallas kernels: 45.9 us -> 42.8 us
    pallas_call x1, Pallas kernels: 43.9 us -> 40.8 us  [fused_body(): pl.pallas_call(layer_kernel, out_shape=(jax.ShapeDtypeStruct((length * he...]
where the time goes in v1:
time: 43.6 us; the launch traced here: 43.4 us
  Pallas kernels  42.8 us (98%)
  between operations  0.64 us (1%)
    pallas_call x1, Pallas kernels, fused_body(): pl.pallas_call(layer_kernel, out_shape=(jax.ShapeDtypeStruct((length * he...  40.8 us
    pallas_call x1, Pallas kernels, fused_body(): pl.pallas_call(hand_on, out_shape=(jax.ShapeDtypeStruct(mix_out.shape, BF...  2.02 us

profile of v1, /device:TPU:0, one launch (start us, length us, event | category | flops | bytes accessed | tf_op | source)
XLA Modules:
  0.0 43.4 jit_solution(12366288226814575574)
XLA Ops:
  0.6 40.8 %shard_map.140 = (bf16[2048,128]{1,0:T(8,128)(2,1)}, bf16[128,1024]{1,0:T(8,128)(2,1)}) custom-call(bf16[2048,128]{1,0:T(8,128)(2,1)} %bitcast.8, bf16[2048,128]{1,0:T(8,128)(2,1)} %bitcast.9, bf16[2048,128]{1,0:T(8,128)(2,1)} %bitcast.10, f32[4,512]{1,0:T(4,128)} %beta_ref.1, f32[4,512]{1,0:T(4,128)} %decay_ref.1, f32[1,128]{1,0:T(1,128)} %bitcast.14, ...), custom_call_target="tpu_custom_call" | custom-call | tf_op jit(solution)/shard_map/pallas_call | solution.py:723
  41.4 2.0 %shard_map.141 = (bf16[2048,128]{1,0:T(8,128)(2,1)}, bf16[128,1024]{1,0:T(8,128)(2,1)}) custom-call(bf16[2048,128]{1,0:T(8,128)(2,1)} %get-tuple-element.6.mix_ref, bf16[128,1024]{1,0:T(8,128)(2,1)} %get-tuple-element.7.ffn_ref), custom_call_target="tpu_custom_call" | custom-call | flops 1000 | bytes 2097152 | tf_op jit(solution)/shard_map/pallas_call | solution.py:785

commit v2 on v1

--- a/solution.py
+++ b/solution.py
@@ -201,61 +201,61 @@
     return lax.broadcasted_iota(jnp.int32, shape, dim)
 
 
-def pair_rows(h, c, chunks):
-    return (h % 2) * chunks + c
-
-
-def state_pair(g, q_ref, k_ref, v_ref, rows_s, cols_s, gp_s, sc_s, wu_s, z_s, m_s, n_s, service):
-    length = k_ref.shape[0]
+def unit_tools(heads, chunks, rows_s, cols_s):
     n = 128
-    chunks = length // n
-    count = 2 * chunks
-    units = [(i, c) for i in range(2) for c in range(chunks)]
+    count = heads * chunks
+
+    def block(ref, u):
+        i, c = u // chunks, u % chunks
+        return ref[c * n : (c + 1) * n, i * n : (i + 1) * n]
+
+    def row_of(kind, u):
+        return rows_s[kind * count + u : kind * count + u + 1, :]
+
+    def col_of(kind, u):
+        return cols_s[:, kind * count + u : kind * count + u + 1]
+
+    return block, row_of, col_of
+
+
+CUM, BETA, DECAY, SUMS, ROOT = range(5)
+
+
+def solve_all(q_ref, k_ref, rows_s, cols_s, qd_s, sc_s, inv_s, service):
+    n = 128
+    heads, chunks = k_ref.shape[1] // n, k_ref.shape[0] // n
+    count = heads * chunks
     row, col = iota((n, n), 0), iota((n, n), 1)
     causal, strict = row >= col, row > col
     same = (row >= n // 2) == (col >= n // 2)
-    eye = (row == col).astype(F32)
-
-    def block(ref, u):
-        i, c = units[u]
-        return ref[c * n : (c + 1) * n, pl.ds(pl.multiple_of((2 * g + i) * n, n), n)]
-
-    def row_of(kind, u):
-        return rows_s[g, kind * count + u : kind * count + u + 1, :]
-
-    def col_of(kind, u):
-        return cols_s[g, :, kind * count + u : kind * count + u + 1]
-
+    inside, outside = strict & same, strict & jnp.logical_not(same)
+    diagonal = row == col
+    eye = diagonal.astype(F32)
+    block, row_of, col_of = unit_tools(heads, chunks, rows_s, cols_s)
     everything = range(count)
-    rks, gathered = [], jnp.zeros((n, n), F32)
+    cum = rows_s[:count, :]
+    rows_s[DECAY * count : (DECAY + 1) * count, :] = jnp.exp(cum)
+    based = cum - jnp.log(rows_s[count : 2 * count, :])
+    cols_s[...] = jnp.transpose(joined([cum, jnp.zeros((n - count, n), F32)], 0))
+    raws = []
     for u in everything:
-        kf = block(k_ref, u).astype(F32)
-        rk = lax.rsqrt(jnp.sum(kf * kf, -1, keepdims=True) + EPSILON)
-        rks.append(rk)
-        gathered = jnp.where(col == u, rk, gathered)
-    rows_s[g, 2 * count : 3 * count, :] = jnp.transpose(gathered)[:count]
-    prods, powers, offs, tails, rowsets = [], [], [], [], []
+        k = block(k_ref, u)
+        raws.append(mm(joined([k, block(q_ref, u)], 0), k, ROWS_ROWS))
+    prods, powers, offs = [], [], []
     for u in everything:
-        i, c = units[u]
-        k, q = block(k_ref, u), block(q_ref, u)
-        qf = q.astype(F32)
-        rq = lax.rsqrt(jnp.sum(qf * qf, -1, keepdims=True) + EPSILON) * (n ** (-0.5))
-        crow, brow, rkrow = row_of(0, u), row_of(1, u), row_of(2, u)
-        ccol, bcol = col_of(0, u), col_of(1, u)
-        raw = mm(joined([k, q], 0), k, ROWS_ROWS)
-        dm = jnp.where(causal, jnp.exp(jnp.where(causal, ccol - crow, 0.0)), 0.0) * rkrow
-        lower = jnp.where(strict, raw[:n] * dm * (rks[u] * bcol), 0.0)
-        sc_s[g, u] = split(raw[n:] * dm * rq)
-        gp_s[g, u] = qf * (rq * jnp.exp(ccol))
-        neg = jnp.where(same, -lower, 0.0)
-        offs.append(jnp.where(same, 0.0, lower))
+        raw, ccol = raws[u], col_of(CUM, u)
+        total = jnp.sum(jnp.where(diagonal, raw[:n], 0.0), 0, keepdims=True) + EPSILON
+        rows_s[SUMS * count + u : SUMS * count + u + 1, :] = total
+        dm = jnp.exp(ccol - (based[u : u + 1] + jnp.log(total)))
+        sc_s[u] = split(jnp.where(causal, raw[n:] * dm, 0.0))
+        qd_s[u] = block(q_ref, u).astype(F32) * jnp.exp(ccol)
+        minus = -raw[:n] * dm
+        neg = jnp.where(inside, minus, 0.0)
+        offs.append(jnp.where(outside, minus, 0.0))
         prods.append(eye + neg)
         powers.append(neg)
-        clast = crow[:, n - 1 :]
-        tails.append((rks[u] * jnp.exp(clast - ccol), jnp.exp(clast)))
-        rowsets.append((brow, brow * rkrow * jnp.exp(crow)))
+    service(0)
     powers = [three(p, p) for p in powers]
-    service(0)
     for turn in range((BLOCK - 1).bit_length() - 2):
         both = [three(joined([a, p], 0), p) for a, p in zip(prods, powers)]
         prods = [a + b[:n] for a, b in zip(prods, both)]
@@ -263,60 +263,91 @@
     service(1)
     prods = [a + three(a, p) for a, p in zip(prods, powers)]
     mids = [three(o, a) for o, a in zip(offs, prods)]
-    prods = [a - three(a, m) for a, m in zip(prods, mids)]
-    pairs = []
+    for u in everything:
+        inv_s[u] = prods[u] + three(prods[u], mids[u])
+    service(2)
+
+
+def advanced(steps, adds, state):
+    sh, sl = halves(state)
+    th, tl = halves(steps)
+    out = mm(joined([th, tl], 1), twice(sh)) + mm(th, sl)
+    return out + joined([jnp.zeros_like(adds), adds], 1)
+
+
+def carry_all(k_ref, v_ref, rows_s, cols_s, inv_s, sc_s, qd_s, y_s, z_s, m_s, n_s):
+    n = 128
+    heads, chunks = k_ref.shape[1] // n, k_ref.shape[0] // n
+    count = heads * chunks
+    eye = (iota((n, n), 0) == iota((n, n), 1)).astype(F32)
+    block, row_of, col_of = unit_tools(heads, chunks, rows_s, cols_s)
+    everything = range(count)
+    totals, cum = rows_s[SUMS * count : (SUMS + 1) * count, :], rows_s[:count, :]
+    rows_s[ROOT * count : (ROOT + 1) * count, :] = jnp.sqrt(totals)
+    tail = rows_s[BETA * count : (BETA + 1) * count, :] / totals * jnp.exp(cum[:, n - 1 :] - cum)
+    cols_s[...] = jnp.transpose(joined([tail, jnp.zeros((n - count, n), F32)], 0))
+    pairs, steps, states, narrow = [], [], [], []
     for u in everything:
         k, v = block(k_ref, u), block(v_ref, u)
-        x, w = prods[u] * rowsets[u][0], prods[u] * rowsets[u][1]
+        solved = inv_s[u]
+        x, w = solved * row_of(ROOT, u), solved * row_of(DECAY, u)
         pairs.append(joined([mm(split(w), twice(k)), mm(split(x), twice(v))], 1))
-        wu_s[g, u] = pairs[u].astype(BF16)
-    service(2)
-    steps = []
     for u in everything:
-        scale, last = tails[u]
-        sh, sl = halves(pairs[u] * scale)
-        k = block(k_ref, u)
-        moved = mm(twice(k), joined([sh, sl], 0), COLS_COLS)
+        narrow.append(pairs[u].astype(BF16))
+        sh, sl = halves(pairs[u] * col_of(0, u))
+        kt = jnp.transpose(block(k_ref, u).astype(F32)).astype(BF16)
+        moved = mm(joined([kt, kt], 1), joined([sh, sl], 0))
+        last = jnp.exp(row_of(CUM, u)[:, n - 1 :])
         steps.append((last * eye - moved[:, :n], moved[:, n:]))
-    states = [None, None]
-    for c in range(chunks):
-        for i in range(2):
-            step, add = steps[i * chunks + c]
-            if c == 0:
-                states[i] = joined([step, add], 1)
-            else:
-                z_s[g, i * (chunks - 1) + c - 1] = states[i].astype(BF16)
-                sh, sl = halves(states[i])
-                th, tl = halves(step)
-                out = mm(joined([th, tl], 1), twice(sh)) + mm(th, sl)
-                states[i] = out + joined([jnp.zeros_like(add), add], 1)
-    for i in range(2):
-        m_s[2 * g + i] = split(states[i][:, :n])
-        n_s[2 * g + i] = states[i][:, n:]
-
-
-def output_pair(g, gp_s, sc_s, wu_s, z_s, gs_s, y_s, chunks):
+
+    def spread_out(units):
+        for u in units:
+            spread = mm(sc_s[u], twice(narrow[u]))
+            sc_s[u] = split(qd_s[u] - spread[:, :n])
+            y_s[u] = spread[:, n:]
+
+    def step_of(i, c):
+        return steps[i * chunks + c]
+
+    first = [joined(step_of(i, 0), 1) for i in range(heads)]
+    if chunks == 4:
+        second = [advanced(*step_of(i, 1), first[i]) for i in range(heads)]
+        upper = [advanced(*step_of(i, 3), joined(step_of(i, 2), 1)) for i in range(heads)]
+        spread_out(everything)
+        third = [advanced(*step_of(i, 2), second[i]) for i in range(heads)]
+        last = [advanced(upper[i][:, :n], upper[i][:, n:], second[i]) for i in range(heads)]
+        states = [first, second, third, last]
+    else:
+        spread_out(everything)
+        states = [first]
+        for c in range(1, chunks):
+            states.append([advanced(*step_of(i, c), states[-1][i]) for i in range(heads)])
+    for i in range(heads):
+        m_s[i] = split(states[-1][i][:, :n])
+        n_s[i] = states[-1][i][:, n:]
+        for c in range(chunks - 1):
+            z_s[i * (chunks - 1) + c] = states[c][i].astype(BF16)
+
+
+def outputs_all(heads, chunks, sc_s, z_s, y_s):
     n = 128
-    count = 2 * chunks
-    spreads = [mm(sc_s[g, u], twice(wu_s[g, u])) for u in range(count)]
-    for u in range(count):
+    for u in range(heads * chunks):
         i, c = u // chunks, u % chunks
-        reader, base = gp_s[g, u] - spreads[u][:, :n], spreads[u][:, n:]
         if c > 0:
-            both = mm(split(reader), twice(z_s[g, i * (chunks - 1) + c - 1]))
-            reader, base = both[:, :n], both[:, n:] + base
-        here = slice(c * n, (c + 1) * n)
-        gs_s[2 * g + i, here, :] = split(reader)
-        y_s[2 * g + i, here, :] = base
+            both = mm(sc_s[u], twice(z_s[i * (chunks - 1) + c - 1]))
+            sc_s[u] = split(both[:, :n])
+            y_s[u] = y_s[u] + both[:, n:]
 
 
 def layer_kernel(
-    q_ref, k_ref, v_ref, beta_ref, decay_ref, ngain_ref, x_ref, gain_ref, ids_ref, share_ref,
-    wg_ref, wu_ref, wd_ref, mix_ref, ffn_ref,
-    q_s, k_s, v_s, flat_s, rows_s, cols_s, sc_s, wu_s, z_s, gp_s, gs_s, y_s, m_s, n_s, sin_s, sout_s,
-    wg_v, wu_v, wd_v, perm_s, disp, info_out, info_all, gall, xall, xe, hmine, hall, place_s, back_s, wide_s, copies_s,
+    q_hbm, k_hbm, v_hbm, beta_hbm, decay_hbm, ngain_hbm, x_hbm, gain_hbm, ids_hbm, share_hbm,
+    wg_ref, wu_ref, wd_ref, mix_hbm, ffn_hbm,
+    mix_ref, ffn_ref, out_sem,
+    q_ref, k_ref, v_ref, beta_ref, decay_ref, ngain_ref, x_ref, gain_ref, ids_ref, share_ref, in_sem,
+    q_s, k_s, v_s, flat_s, rows_s, cols_s, sc_s, z_s, qd_s, inv_s, y_s, m_s, n_s, sin_s, sout_s,
+    wg_v, wu_v, wd_v, perm_s, disp, info_out, info_all, sq_all, sc_out, sc_all, gall, xall, xw_s, gacc_s, uacc_s, hmine, hall, place_s, back_s, dacc_s, copies_s,
     ret_out, ret_in,
-    w_sem, d_send, d_recv, i_send, i_recv, g_send, g_recv,
+    w_sem, d_send, d_recv, i_send, i_recv, g_send, g_recv, q_send, q_recv, t_send, t_recv,
     gx_send, gx_recv, gc_send, gc_recv, hx_send, hx_recv, hc_send, hc_recv,
     r_send, r_recv, c_send, c_recv,
 ):
@@ -333,6 +364,14 @@
     parts = r_send.shape[1]
     wide_part = ffn_ref.shape[1] // parts
 
+    def nearest(k):
+        left, right = me, ep - 1 - me
+        inner = jnp.minimum(left, right)
+        both = k < 2 * inner
+        far = jnp.where(both, k // 2 + 1, k - inner + 1)
+        upward = jnp.where(both, k % 2, jnp.where(right > left, 0, 1)) == 0
+        return jnp.where(upward, me + far, me - far)
+
     def away(axis, count, mine, step):
         return {axis: lax.rem(mine + step, count)}
 
@@ -352,9 +391,18 @@
         src, dst = ((wg_ref, wg_v), (wu_ref, wu_v), (wd_ref, wd_v))[which]
         return pltpu.make_async_copy(src.at[e], dst.at[e], w_sem.at[which, e])
 
-    for which in range(3):
-        for e in range(local):
-            weight(which, e).start()
+    arriving = [
+        pltpu.make_async_copy(src, dst, in_sem.at[i])
+        for i, (src, dst) in enumerate((
+            (ids_hbm, ids_ref), (x_hbm, x_ref), (share_hbm, share_ref), (gain_hbm, gain_ref),
+            (k_hbm, k_ref), (v_hbm, v_ref), (q_hbm, q_ref),
+            (beta_hbm, beta_ref), (decay_hbm, decay_ref), (ngain_hbm, ngain_ref),
+        ))
+    ]
+    for copy in arriving:
+        copy.start()
+    for copy in arriving[:4]:
+        copy.wait()
 
     ids = ids_ref[...]
     first = ids[0:1]
@@ -381,12 +429,15 @@
     info_out[...] = info
     info_all[me] = info
     gall[mt] = gain_ref[...]
+    sorted_rows = disp[...].astype(F32)
+    sums = jnp.sum(sorted_rows * sorted_rows, -1, keepdims=True)
+    sq_all[mt] = jnp.transpose(jnp.broadcast_to(sums, (tokens, tokens)))[:8]
     xall[mt, pl.ds(pl.multiple_of(me * cap, cap), cap), :] = disp[
         pl.ds(pl.multiple_of(me * cap, cap), cap), :
     ]
 
     def dispatch(step):
-        to = lax.rem(me + step, ep)
+        to = nearest(step - 1)
         return remote(
             disp.at[pl.ds(pl.multiple_of(to * cap, cap), cap)],
             xall.at[mt, pl.ds(pl.multiple_of(me * cap, cap), cap)],
@@ -394,12 +445,32 @@
         )
 
     def tell(step):
-        to = lax.rem(me + step, ep)
+        to = nearest(step - 1)
         return remote(info_out, info_all.at[me], i_send.at[to], i_recv.at[me], {"ep": to})
 
     def gains(step):
         to = lax.rem(mt + step, tp)
         return remote(gain_ref, gall.at[mt], g_send.at[to], g_recv.at[mt], {"tp": to})
+
+    def squares(step):
+        to = lax.rem(mt + step, tp)
+        return remote(sq_all.at[mt], sq_all.at[mt], q_send.at[to], q_recv.at[mt], {"tp": to})
+
+    def scales(step):
+        to = nearest(step - 1)
+        return remote(sc_out, sc_all.at[me], t_send.at[to], t_recv.at[me], {"ep": to})
+
+    def send_scales():
+        total = sq_all[mt]
+        for step in range(1, tp):
+            t = lax.rem(mt + step, tp)
+            landed(sq_all.at[t], q_recv.at[t])
+            total = total + sq_all[t]
+        row = lax.rsqrt(total / (tp * dl) + EPSILON)
+        sc_out[...] = row
+        sc_all[me] = row
+        for step in range(1, ep):
+            scales(step).start()
 
     def chunk_of(origin, s):
         return xall.at[origin, pl.ds(pl.multiple_of(s * cap, cap), cap)]
@@ -437,7 +508,7 @@
             h_to_mate(step, e).start()
 
     def giving(step, part):
-        to = lax.rem(me + step, ep)
+        to = nearest(ep - 1 - step)
         lanes = slice(part * wide_part, (part + 1) * wide_part)
         return remote(
             ret_out.at[pl.ds(pl.multiple_of(to * cap, cap), cap), lanes],
@@ -448,7 +519,15 @@
     def landed(dst, sem):
         pltpu.make_async_copy(dst, dst, sem).wait()
 
+    for copy in arriving[4:]:
+        copy.wait()
+    for which in range(3):
+        for e in range(local):
+            weight(which, e).start()
+
     pl.semaphore_wait(barrier, ep - 1 + tp - 1)
+    for step in range(1, tp):
+        squares(step).start()
     for step in range(1, ep):
         dispatch(step).start()
         tell(step).start()
@@ -456,7 +535,7 @@
         gains(step).start()
 
     def forward(j):
-        s = lax.rem(me + j, ep)
+        s = nearest(j - 1) if j > 0 else me
         if j > 0:
             landed(chunk_of(mt, s), d_recv.at[s])
         for step in range(1, chips):
@@ -464,13 +543,12 @@
         to_mate(0, s).start()
 
     def relay(j):
-        s = lax.rem(me + j, ep)
+        s = nearest(j - 1) if j > 0 else me
         for step in range(1, chips):
             origin = lax.rem(chip + step, chips)
             landed(chunk_of(origin * 2 + core, s), gx_recv.at[origin, s])
             to_mate(step, s).start()
 
-    order = [j for near in range(1, ep // 2 + 1) for j in sorted({near, ep - near})]
     forward(0)
 
     for src, dst in ((k_ref, k_s), (v_ref, v_s), (q_ref, q_s)):
@@ -497,45 +575,21 @@
         here = slice(c * 128, (c + 1) * 128)
         summed = -exact(rates[:, here], ones_upper)
         for h in range(heads):
-            u = pair_rows(h, c, chunks)
-            rows_s[h // 2, u : u + 1, :] = summed[h : h + 1]
-            rows_s[h // 2, 2 * chunks + u : 2 * chunks + u + 1, :] = strengths[h : h + 1, here]
-    for g in range(heads // 2):
-        cols_s[g] = jnp.transpose(rows_s[g])
+            u = h * chunks + c
+            rows_s[u : u + 1, :] = summed[h : h + 1]
+            rows_s[heads * chunks + u : heads * chunks + u + 1, :] = strengths[h : h + 1, here]
 
     def chain_copy(h):
         return remote(sout_s.at[h], sin_s.at[h], c_send.at[h], c_recv.at[h], {"ep": lax.rem(me + 1, ep)})
 
-    def one_pair(g, carry):
-        def service(place):
-            if place == 1:
-                @pl.when(g == 0)
-                def _():
-                    for j in order[:-1]:
-                        forward(j)
-
-                @pl.when(g == 1)
-                def _():
-                    for j in order[:-1]:
-                        relay(j)
-
-        state_pair(g, q_s, k_s, v_s, rows_s, cols_s, gp_s, sc_s, wu_s, z_s, m_s, n_s, service)
+    def carry_on():
+        carry_all(k_s, v_s, rows_s, cols_s, inv_s, sc_s, qd_s, y_s, z_s, m_s, n_s)
 
         @pl.when(me == 0)
         def _():
-            for i in range(2):
-                sout_s[2 * g + i] = n_s[2 * g + i].astype(BF16)
-                chain_copy(2 * g + i).start()
-
-        @pl.when(g == 0)
-        def _():
-            relay(0)
-            forward(order[-1])
-
-        return carry
-
-    lax.fori_loop(0, heads // 2, one_pair, 0)
-    relay(order[-1])
+            for h in range(heads):
+                sout_s[h] = n_s[h].astype(BF16)
+                chain_copy(h).start()
 
     def chain_turn(low, high):
         def turn(h, carry):
@@ -553,24 +607,36 @@
 
         return all_turns
 
-    def outputs(low, high):
-        def one(h, carry):
-            output_pair(h, gp_s, sc_s, wu_s, z_s, gs_s, y_s, chunks)
-            return carry
-
-        lax.fori_loop(low, high, one, 0)
-
-    last = heads - 1
-    pl.when(me == 1)(chain_turn(0, last))
+    def outputs():
+        outputs_all(heads, length // 128, sc_s, z_s, y_s)
+
+    def early(place):
+        if place == 0:
+            send_scales()
+        elif place == 1:
+            for j in range(1, ep - 1):
+                forward(j)
+        elif place == 2:
+            forward(ep - 1)
+            relay(0)
+
+    solve_all(q_s, k_s, rows_s, cols_s, qd_s, sc_s, inv_s, early)
+    carry_on()
+    for j in range(1, ep - 1):
+        relay(j)
 
     for step in range(1, ep):
         s = lax.rem(me + step, ep)
         landed(info_all.at[s], i_recv.at[s])
-    r_in, r_out = iota((tokens, tokens), 0), iota((tokens, tokens), 1)
-    told = jnp.zeros((n_rows, tokens), F32)
-    for s in range(ep):
-        take = (r_in - me * cap == r_out - s * cap) & (r_out >= s * cap) & (r_out < (s + 1) * cap)
-        told = told + exact(info_all[s], take.astype(F32))
+    r_in, r_out = iota((ep * tokens, tokens), 0), iota((ep * tokens, tokens), 1)
+    source = r_in // tokens
+    takes = (r_in - source * tokens - me * cap == r_out - source * cap) & (r_out // cap == source)
+    takes = takes.astype(F32).astype(BF16)
+    left, told = joined([info_all[s] for s in range(ep)], 1), jnp.zeros((n_rows, tokens), F32)
+    for piece in range(3):
+        taken = left.astype(BF16)
+        told = told + mm(taken, takes)
+        left = left - taken.astype(F32)
     ranks = mm(told.astype(BF16), upper)
     for e in range(local):
         where_to = iota((cap_e, tokens), 0).astype(F32) == ranks[e : e + 1]
@@ -582,86 +648,132 @@
             back_s[piece, :, e * cap_e : (e + 1) * cap_e] = taken
             left = left - taken.astype(F32)
 
+
+    relay(ep - 1)
+    for step in range(1, ep):
+        s = lax.rem(me + step, ep)
+        landed(sc_all.at[s], t_recv.at[s])
+    left, row = joined([sc_all[s] for s in range(ep)], 1), jnp.zeros((8, tokens), F32)
+    for piece in range(3):
+        taken = left.astype(BF16)
+        row = row + mm(taken, takes)
+        left = left - taken.astype(F32)
+    scale = jnp.transpose(jnp.broadcast_to(row[:1], (tokens, tokens)))[:, :1]
     for step in range(1, tp):
         t = lax.rem(mt + step, tp)
         landed(gall.at[t], g_recv.at[t])
-    for step in range(chips):
-        origin = lax.rem(chip + step, chips)
+
+    def origin_of(step):
+        return lax.rem(chip + step, chips)
+
+    def weights_of(step):
+        return pl.ds(pl.multiple_of(origin_of(step) * 2 * dl, 2 * dl), 2 * dl)
+
+    def gained(step):
+        for side in range(2):
+            t = origin_of(step) * 2 + side
+            xw_s[:, side * dl : (side + 1) * dl] = (xall[t].astype(F32) * scale * gall[t]).astype(BF16)
+
+    def mates(step):
         for s in range(ep):
-            landed(chunk_of(origin * 2 + 1 - core, s), gc_recv.at[origin, s])
-
-    def squares(t, total):
-        part = xall[t].astype(F32)
-        return total + jnp.sum(part * part, -1, keepdims=True)
-
-    total = lax.fori_loop(0, tp, squares, jnp.zeros((tokens, 1), F32))
-    scale = lax.rsqrt(total / (tp * dl) + EPSILON)
-
-    def spread_rows(t, carry):
-        normed = (xall[t].astype(F32) * scale * gall[t]).astype(BF16)
-        xe[:, pl.ds(pl.multiple_of(t * dl, dl), dl)] = mm(place_s[...], normed).astype(BF16)
-        return carry
-
-    lax.fori_loop(0, tp, spread_rows, 0)
-
-    def one_expert(e, carry):
-        rows = pl.ds(pl.multiple_of(e * cap_e, cap_e), cap_e)
+            landed(chunk_of(origin_of(step) * 2 + 1 - core, s), gc_recv.at[origin_of(step), s])
+
+    mates(0)
+    gained(0)
+
+    for e in range(local):
         weight(0, e).wait()
         weight(1, e).wait()
-        gate = mm(xe[rows, :], wg_v[e])
-        up = mm(xe[rows, :], wu_v[e])
+    for e in range(local):
+        gacc_s[e] = mm(xw_s[...], wg_v[e, weights_of(0), :])
+        uacc_s[e] = mm(xw_s[...], wu_v[e, weights_of(0), :])
+    outputs()
+    for step in range(1, chips - 1):
+        mates(step)
+        gained(step)
+        for e in range(local):
+            gacc_s[e] = gacc_s[e] + mm(xw_s[...], wg_v[e, weights_of(step), :])
+            uacc_s[e] = uacc_s[e] + mm(xw_s[...], wu_v[e, weights_of(step), :])
+    mates(chips - 1)
+    gained(chips - 1)
+
+    def sums(e):
+        part = weights_of(chips - 1)
+        return gacc_s[e] + mm(xw_s[...], wg_v[e, part, :]), uacc_s[e] + mm(xw_s[...], wu_v[e, part, :])
+
+    following = sums(0)
+    for e in range(local):
+        rows = expert_rows(e)
+        gate, up = following
+        if e + 1 < local:
+            following = sums(e + 1)
         hidden = (gate / (1.0 + jnp.exp(-gate)) * up).astype(BF16)
+        hidden = mm(place_s[rows, :], hidden).astype(BF16)
         hmine[rows, :] = hidden
         hall[mt, rows, :] = hidden
         for step in range(1, chips):
             h_over_x(step, e).start()
         h_to_mate(0, e).start()
-        return carry
-
-    lax.fori_loop(0, local, one_expert, 0)
-    h_relay(0)
-    pl.when(me == 1)(chain_turn(last, heads))
-    pl.when(me == 2)(chain_turn(0, last))
-    outputs(0, 1)
-    for e in range(1, local):
-        h_relay(e)
-    pl.when(me == 2)(chain_turn(last, heads))
-    pl.when(me >= 3)(chain_turn(0, last))
-    for e in range(local):
-        for step in range(chips):
-            origin = lax.rem(chip + step, chips)
-            landed(hall.at[origin * 2 + 1 - core, expert_rows(e)], hc_recv.at[origin, e])
+
+    pl.when(me == 1)(chain_turn(0, heads))
+
+    def finals():
+        for u in range(heads * chunks):
+            h, c = u // chunks, u % chunks
+            mixed = mm(sc_s[u], twice(sin_s[h])) + y_s[u]
+            query = q_s[c * 128 : (c + 1) * 128, h * 128 : (h + 1) * 128].astype(F32)
+            squared = jnp.sum(query * query, -1, keepdims=True) + EPSILON
+            rq = lax.rsqrt(squared) * (128 ** (-0.5))
+            factor = rq * lax.rsqrt(jnp.mean(mixed * mixed, -1, keepdims=True) * (rq * rq) + EPSILON)
+            flat_s[pl.ds(c * 128 * heads + h, 128, stride=heads), :] = mixed * factor * ngain_ref[...]
+        mix_ref[...] = flat_s[...].astype(BF16)
+
+    @pl.when(me == 0)
+    def _():
+        sin_s[...] = jnp.zeros_like(sin_s)
+
+    units = 2 * hall.shape[2]
+
+    def hidden_of(step, e):
+        rows = expert_rows(e)
+        landed(hall.at[origin_of(step) * 2 + 1 - core, rows], hc_recv.at[origin_of(step), e])
+        return joined([hall[origin_of(step) * 2 + side, rows, :] for side in range(2)], 1)
+
+    def downs(step, e):
+        return wd_v[e, pl.ds(pl.multiple_of(origin_of(step) * units, units), units), :]
 
     for e in range(local):
         weight(2, e).wait()
+    for e in range(local // 2):
+        h_relay(e)
+    for step in range(chips - 1):
+        for e in range(local):
+            rows = slice(e * cap_e, (e + 1) * cap_e)
+            out = mm(hidden_of(step, e), downs(step, e))
+            dacc_s[rows, :] = out if step == 0 else dacc_s[rows, :] + out
+    for e in range(local // 2, local):
+        h_relay(e)
+    pl.when(me == 2)(chain_turn(0, heads))
+    for e in range(local):
+        rows = slice(e * cap_e, (e + 1) * cap_e)
+        out = dacc_s[rows, :] + mm(hidden_of(chips - 1, e), downs(chips - 1, e))
+        copies_s[rows, :] = out.astype(BF16)
     own = pl.ds(pl.multiple_of(me * cap, cap), cap)
-    for t in range(tp):
-        wide_s[:, t * hall.shape[2] : (t + 1) * hall.shape[2]] = hall[t]
     for part in range(parts):
         lanes = slice(part * wide_part, (part + 1) * wide_part)
-        for e in range(local):
-            rows = slice(e * cap_e, (e + 1) * cap_e)
-            copies_s[rows, lanes] = mm(wide_s[rows, :], wd_v[e, :, lanes]).astype(BF16)
-        result = mm(back_s[0], copies_s[:, lanes])
-        for piece in range(1, back_s.shape[0]):
-            result = result + mm(back_s[piece], copies_s[:, lanes])
+        result = mm(joined([back_s[piece] for piece in range(back_s.shape[0])], 1), twice(copies_s[:, lanes]))
         ret_out[:, lanes] = result.astype(BF16)
         ret_in[own, lanes] = ret_out[own, lanes]
         for step in range(1, ep):
             giving(step, part).start()
 
-    outputs(1, heads // 2)
-    pl.when(me >= 3)(chain_turn(last, heads))
-
-    @pl.when(me == 0)
-    def _():
-        sin_s[...] = jnp.zeros_like(sin_s)
-
-    for h in range(heads):
-        mixed = mm(gs_s[h], twice(sin_s[h])) + y_s[h]
-        normed = mixed * lax.rsqrt(jnp.mean(mixed * mixed, -1, keepdims=True) + EPSILON)
-        flat_s[pl.ds(h, length, stride=heads), :] = normed * ngain_ref[...]
-    mix_ref[...] = flat_s[...].astype(BF16)
+    pl.when(me >= 3)(chain_turn(0, heads))
+    finals()
+    written = (
+        pltpu.make_async_copy(mix_ref, mix_hbm, out_sem.at[0]),
+        pltpu.make_async_copy(ffn_ref, ffn_hbm, out_sem.at[1]),
+    )
+    written[0].start()
 
     for step in range(1, ep):
         s = lax.rem(me + step, ep)
@@ -669,14 +781,17 @@
             lanes = slice(part * wide_part, (part + 1) * wide_part)
             landed(ret_in.at[pl.ds(pl.multiple_of(s * cap, cap), cap), lanes], r_recv.at[s, part])
     ffn_ref[...] = mm(perm_s[...], ret_in[...], COLS_COLS).astype(BF16)
+    written[1].start()
 
     for step in range(1, ep):
         dispatch(step).wait_send()
+        scales(step).wait_send()
         tell(step).wait_send()
         for part in range(parts):
             giving(step, part).wait_send()
     for step in range(1, tp):
         gains(step).wait_send()
+        squares(step).wait_send()
     for step in range(1, chips):
         for e in range(local):
             h_over_x(step, e).wait_send()
@@ -695,6 +810,9 @@
             return carry
 
         lax.fori_loop(0, heads, sent, 0)
+
+    for copy in written:
+        copy.wait()
 
 
 def hand_on(mix_ref, ffn_ref, mix_out, ffn_out):
@@ -718,29 +836,41 @@
     parts = max(1, min(2, out_width // 512))
     dma = pltpu.SemaphoreType.DMA
     vmem = pl.BlockSpec(memory_space=pltpu.VMEM)
-    hbm = pl.BlockSpec(memory_space=pl.ANY)
-    pairs, chunks = heads // 2, length // width
+    units = heads * (length // width)
     mix_out, ffn_out = pl.pallas_call(
         layer_kernel,
         out_shape=(
             jax.ShapeDtypeStruct((length * heads, width), BF16),
             jax.ShapeDtypeStruct((tokens, out_width), BF16),
         ),
-        in_specs=[vmem] * 10 + [hbm] * 3,
-        out_specs=(vmem, vmem),
+        in_specs=[pl.BlockSpec(memory_space=pltpu.HBM)] * 13,
+        out_specs=(pl.BlockSpec(memory_space=pltpu.HBM),) * 2,
         scratch_shapes=[
+            pltpu.VMEM((length * heads, width), BF16),
+            pltpu.VMEM((tokens, out_width), BF16),
+            dma((2,)),
+            pltpu.VMEM((length * heads, width), BF16),
+            pltpu.VMEM((length * heads, width), BF16),
+            pltpu.VMEM((length * heads, width), BF16),
+            pltpu.VMEM(beta_in.shape, F32),
+            pltpu.VMEM(decay_in.shape, F32),
+            pltpu.VMEM((1, width), F32),
+            pltpu.VMEM(ffn_input.shape, BF16),
+            pltpu.VMEM((1, dl), F32),
+            pltpu.VMEM((picks, tokens), jnp.int32),
+            pltpu.VMEM((picks, tokens), F32),
+            dma((10,)),
             pltpu.VMEM((length, heads * width), BF16),
             pltpu.VMEM((length, heads * width), BF16),
             pltpu.VMEM((length, heads * width), BF16),
             pltpu.VMEM((length * heads, width), F32),
-            pltpu.VMEM((pairs, 128, 128), F32),
-            pltpu.VMEM((pairs, 128, 128), F32),
-            pltpu.VMEM((pairs, 2 * chunks, width, 2 * width), BF16),
-            pltpu.VMEM((pairs, 2 * chunks, width, 2 * width), BF16),
-            pltpu.VMEM((pairs, max(2 * (chunks - 1), 1), width, 2 * width), BF16),
-            pltpu.VMEM((pairs, 2 * chunks, width, width), F32),
-            pltpu.VMEM((heads, length, 2 * width), BF16),
-            pltpu.VMEM((heads, length, width), F32),
+            pltpu.VMEM((128, 128), F32),
+            pltpu.VMEM((128, 128), F32),
+            pltpu.VMEM((units, width, 2 * width), BF16),
+            pltpu.VMEM((max(units - heads, 1), width, 2 * width), BF16),
+            pltpu.VMEM((units, width, width), F32),
+            pltpu.VMEM((units, width, width), F32),
+            pltpu.VMEM((units, width, width), F32),
             pltpu.VMEM((heads, width, 2 * width), BF16),
             pltpu.VMEM((heads, width, width), F32),
             pltpu.VMEM((heads, width, width), BF16),
@@ -752,20 +882,26 @@
             pltpu.VMEM((tokens, dl), BF16),
             pltpu.VMEM((n_rows, tokens), F32),
             pltpu.VMEM((ep, n_rows, tokens), F32),
+            pltpu.VMEM((tp, 8, tokens), F32),
+            pltpu.VMEM((8, tokens), F32),
+            pltpu.VMEM((ep, 8, tokens), F32),
             pltpu.VMEM((tp, 1, dl), F32),
             pltpu.VMEM((tp, tokens, dl), BF16),
-            pltpu.VMEM((rows_e, full), BF16),
+            pltpu.VMEM((tokens, full // chips), BF16),
+            pltpu.VMEM((local, tokens, fl), F32),
+            pltpu.VMEM((local, tokens, fl), F32),
             pltpu.VMEM((rows_e, fl), BF16),
             pltpu.VMEM((tp, rows_e, fl), BF16),
             pltpu.VMEM((rows_e, tokens), BF16),
-            pltpu.VMEM((3, tokens, rows_e), BF16),
-            pltpu.VMEM((rows_e, tp * fl), BF16),
+            pltpu.VMEM((2, tokens, rows_e), BF16),
+            pltpu.VMEM((rows_e, out_width), F32),
             pltpu.VMEM((rows_e, out_width), BF16),
             pltpu.VMEM((tokens, out_width), BF16),
             pltpu.VMEM((tokens, out_width), BF16),
             dma((3, local)),
             dma((ep,)), dma((ep,)), dma((ep,)), dma((ep,)),
-            dma((tp,)), dma((tp,)),
+            dma((tp,)), dma((tp,)), dma((tp,)), dma((tp,)),
+            dma((ep,)), dma((ep,)),
             dma((chips, ep)), dma((chips, ep)), dma((chips, ep)), dma((chips, ep)),
             dma((chips, local)), dma((chips, local)), dma((chips, local)), dma((chips, local)),
             dma((ep, parts)), dma((ep, parts)),
@@ -813,7 +949,8 @@
     width, local = mix_query.shape[2], w_gate.shape[0]
     whole_groups = local % GROUP == 0 and expert_ids.shape[1] == 2
     even = lax.axis_size("tp") % 2 == 0 and lax.axis_size("tp") > 1 and lax.axis_size("ep") > 1
-    if whole_groups and even and mix_query.shape[1] == 4 and width == 128 and mix_query.shape[0] % 128 == 0:
+    units = mix_query.shape[1] * mix_query.shape[0] // 128
+    if whole_groups and even and units % 8 == 0 and units < 25 and width == 128 and mix_query.shape[0] % 128 == 0:
         return fused_body(
             mix_query,
             mix_keys,

time: 43.6 us -> 38.8 us (0.89)
  Pallas kernels: 42.8 us -> 38 us
    pallas_call x1, Pallas kernels: 40.8 us -> 36 us  [fused_body(): pl.pallas_call(layer_kernel, out_shape=(jax.ShapeDtypeStruct((length * he...]
where the time goes in v2:
time: 38.8 us; the launch traced here: 38.6 us
  Pallas kernels  38 us (98%)
  between operations  0.64 us (2%)
    pallas_call x1, Pallas kernels, fused_body(): pl.pallas_call(layer_kernel, out_shape=(jax.ShapeDtypeStruct((length * he...  36 us
    pallas_call x1, Pallas kernels, fused_body(): pl.pallas_call(hand_on, out_shape=(jax.ShapeDtypeStruct(mix_out.shape, BF...  2.02 us

profile of v2, /device:TPU:0, one launch (start us, length us, event | category | flops | bytes accessed | tf_op | source)
XLA Modules:
  0.0 38.6 jit_solution(17196652113419959592)
XLA Ops:
  0.6 36.0 %shard_map.140 = (bf16[2048,128]{1,0:T(8,128)(2,1)}, bf16[128,1024]{1,0:T(8,128)(2,1)}) custom-call(bf16[2048,128]{1,0:T(8,128)(2,1)} %bitcast.8, bf16[2048,128]{1,0:T(8,128)(2,1)} %bitcast.9, bf16[2048,128]{1,0:T(8,128)(2,1)} %bitcast.10, f32[4,512]{1,0:T(4,128)} %beta_hbm.1, f32[4,512]{1,0:T(4,128)} %decay_hbm.1, f32[1,128]{1,0:T(1,128)} %bitcast.14, ...), custom_call_target="tpu_custom_call" | custom-call | tf_op jit(solution)/shard_map/pallas_call | solution.py:840
  36.6 2.0 %shard_map.141 = (bf16[2048,128]{1,0:T(8,128)(2,1)}, bf16[128,1024]{1,0:T(8,128)(2,1)}) custom-call(bf16[2048,128]{1,0:T(8,128)(2,1)} %get-tuple-element.6.mix_ref, bf16[128,1024]{1,0:T(8,128)(2,1)} %get-tuple-element.7.ffn_ref), custom_call_target="tpu_custom_call" | custom-call | flops 1000 | bytes 2097152 | tf_op jit(solution)/shard_map/pallas_call | solution.py:921

commit v3 on v2

--- a/solution.py
+++ b/solution.py
@@ -341,8 +341,7 @@
 
 def layer_kernel(
     q_hbm, k_hbm, v_hbm, beta_hbm, decay_hbm, ngain_hbm, x_hbm, gain_hbm, ids_hbm, share_hbm,
-    wg_ref, wu_ref, wd_ref, mix_hbm, ffn_hbm,
-    mix_ref, ffn_ref, out_sem,
+    wg_ref, wu_ref, wd_ref, mix_ref, ffn_ref,
     q_ref, k_ref, v_ref, beta_ref, decay_ref, ngain_ref, x_ref, gain_ref, ids_ref, share_ref, in_sem,
     q_s, k_s, v_s, flat_s, rows_s, cols_s, sc_s, z_s, qd_s, inv_s, y_s, m_s, n_s, sin_s, sout_s,
     wg_v, wu_v, wd_v, perm_s, disp, info_out, info_all, sq_all, sc_out, sc_all, gall, xall, xw_s, gacc_s, uacc_s, hmine, hall, place_s, back_s, dacc_s, copies_s,
@@ -611,19 +610,16 @@
         outputs_all(heads, length // 128, sc_s, z_s, y_s)
 
     def early(place):
-        if place == 0:
+        if place == 1:
             send_scales()
-        elif place == 1:
-            for j in range(1, ep - 1):
+            forward(1)
+        elif place == 2:
+            for j in range(2, ep):
                 forward(j)
-        elif place == 2:
-            forward(ep - 1)
             relay(0)
 
     solve_all(q_s, k_s, rows_s, cols_s, qd_s, sc_s, inv_s, early)
     carry_on()
-    for j in range(1, ep - 1):
-        relay(j)
 
     for step in range(1, ep):
         s = lax.rem(me + step, ep)
@@ -649,7 +645,9 @@
             left = left - taken.astype(F32)
 
 
-    relay(ep - 1)
+    outputs()
+    for j in range(1, ep):
+        relay(j)
     for step in range(1, ep):
         s = lax.rem(me + step, ep)
         landed(sc_all.at[s], t_recv.at[s])
@@ -687,7 +685,6 @@
     for e in range(local):
         gacc_s[e] = mm(xw_s[...], wg_v[e, weights_of(0), :])
         uacc_s[e] = mm(xw_s[...], wu_v[e, weights_of(0), :])
-    outputs()
     for step in range(1, chips - 1):
         mates(step)
         gained(step)
@@ -744,14 +741,12 @@
 
     for e in range(local):
         weight(2, e).wait()
-    for e in range(local // 2):
-        h_relay(e)
     for step in range(chips - 1):
         for e in range(local):
             rows = slice(e * cap_e, (e + 1) * cap_e)
             out = mm(hidden_of(step, e), downs(step, e))
             dacc_s[rows, :] = out if step == 0 else dacc_s[rows, :] + out
-    for e in range(local // 2, local):
+    for e in range(local):
         h_relay(e)
     pl.when(me == 2)(chain_turn(0, heads))
     for e in range(local):
@@ -769,19 +764,12 @@
 
     pl.when(me >= 3)(chain_turn(0, heads))
     finals()
-    written = (
-        pltpu.make_async_copy(mix_ref, mix_hbm, out_sem.at[0]),
-        pltpu.make_async_copy(ffn_ref, ffn_hbm, out_sem.at[1]),
-    )
-    written[0].start()
-
     for step in range(1, ep):
         s = lax.rem(me + step, ep)
         for part in range(parts):
             lanes = slice(part * wide_part, (part + 1) * wide_part)
             landed(ret_in.at[pl.ds(pl.multiple_of(s * cap, cap), cap), lanes], r_recv.at[s, part])
     ffn_ref[...] = mm(perm_s[...], ret_in[...], COLS_COLS).astype(BF16)
-    written[1].start()
 
     for step in range(1, ep):
         dispatch(step).wait_send()
@@ -811,13 +799,16 @@
 
         lax.fori_loop(0, heads, sent, 0)
 
-    for copy in written:
+
+def hand_on(mix_ref, ffn_ref, mix_out, ffn_out, sems):
+    copies = [
+        pltpu.make_async_copy(mix_ref, mix_out, sems.at[0]),
+        pltpu.make_async_copy(ffn_ref, ffn_out, sems.at[1]),
+    ]
+    for copy in copies:
+        copy.start()
+    for copy in copies:
         copy.wait()
-
-
-def hand_on(mix_ref, ffn_ref, mix_out, ffn_out):
-    mix_out[...] = mix_ref[...]
-    ffn_out[...] = ffn_ref[...]
 
 
 def fused_body(
@@ -840,15 +831,12 @@
     mix_out, ffn_out = pl.pallas_call(
         layer_kernel,
         out_shape=(
-            jax.ShapeDtypeStruct((length * heads, width), BF16),
-            jax.ShapeDtypeStruct((tokens, out_width), BF16),
+            pltpu.VMEM((length * heads, width), BF16),
+            pltpu.VMEM((tokens, out_width), BF16),
         ),
         in_specs=[pl.BlockSpec(memory_space=pltpu.HBM)] * 13,
-        out_specs=(pl.BlockSpec(memory_space=pltpu.HBM),) * 2,
+        out_specs=(vmem, vmem),
         scratch_shapes=[
-            pltpu.VMEM((length * heads, width), BF16),
-            pltpu.VMEM((tokens, out_width), BF16),
-            dma((2,)),
             pltpu.VMEM((length * heads, width), BF16),
             pltpu.VMEM((length * heads, width), BF16),
             pltpu.VMEM((length * heads, width), BF16),
@@ -925,8 +913,10 @@
             jax.ShapeDtypeStruct(ffn_out.shape, BF16),
         ),
         in_specs=[vmem] * 2,
-        out_specs=(vmem, vmem),
+        out_specs=(pl.BlockSpec(memory_space=pltpu.HBM),) * 2,
+        scratch_shapes=[dma((2,))],
         cost_estimate=pl.CostEstimate(flops=1000, bytes_accessed=2**21, transcendentals=0),
+        compiler_params=pltpu.CompilerParams(vmem_limit_bytes=4 * 1024 * 1024),
     )(mix_out, ffn_out)
     return (mix_out.reshape(length, heads, width), ffn_out)
 

time: 38.8 us -> 35.7 us (0.920)
  Pallas kernels: 38 us -> 34.7 us
    pallas_call x1, Pallas kernels: 36 us -> 33.8 us  [fused_body(): pl.pallas_call(layer_kernel, out_shape=(pltpu.VMEM((length * heads, width...]
    pallas_call x1, Pallas kernels: 2.02 us -> 0.89 us  [fused_body(): pl.pallas_call(hand_on, out_shape=(jax.ShapeDtypeStruct(mix_out.shape, BF...]
where the time goes in v3:
time: 35.7 us; the launch traced here: 35.5 us
  Pallas kernels  34.7 us (97%)
  between operations  0.8 us (2%)
    pallas_call x1, Pallas kernels, fused_body(): pl.pallas_call(layer_kernel, out_shape=(pltpu.VMEM((length * heads, width...  33.8 us
    pallas_call x1, Pallas kernels, fused_body(): pl.pallas_call(hand_on, out_shape=(jax.ShapeDtypeStruct(mix_out.shape, BF...  0.89 us

profile of v3, /device:TPU:0, one launch (start us, length us, event | category | flops | bytes accessed | tf_op | source)
XLA Modules:
  0.0 35.5 jit_solution(9445501525264796656)
XLA Ops:
  0.6 33.8 %shard_map.140 = (bf16[2048,128]{1,0:T(8,128)(2,1)S(1)}, bf16[128,1024]{1,0:T(8,128)(2,1)S(1)}) custom-call(bf16[2048,128]{1,0:T(8,128)(2,1)} %bitcast.8, bf16[2048,128]{1,0:T(8,128)(2,1)} %bitcast.9, bf16[2048,128]{1,0:T(8,128)(2,1)} %bitcast.10, f32[4,512]{1,0:T(4,128)} %beta_hbm.1, f32[4,512]{1,0:T(4,128)} %decay_hbm.1, f32[1,128]{1,0:T(1,128)} %bitcast.14, ...), custom_call_target="tpu_custom_call" | custom-call | tf_op jit(solution)/shard_map/pallas_call | solution.py:831
  34.5 0.9 %shard_map.141 = (bf16[2048,128]{1,0:T(8,128)(2,1)}, bf16[128,1024]{1,0:T(8,128)(2,1)}) custom-call(bf16[2048,128]{1,0:T(8,128)(2,1)S(1)} %get-tuple-element.6.mix_ref, bf16[128,1024]{1,0:T(8,128)(2,1)S(1)} %get-tuple-element.7.ffn_ref), custom_call_target="tpu_custom_call" | custom-call | flops 1000 | bytes 2097152 | tf_op jit(solution)/shard_map/pallas_call | solution.py:909

commit v4 on v3

--- a/solution.py
+++ b/solution.py
@@ -645,7 +645,6 @@
             left = left - taken.astype(F32)
 
 
-    outputs()
     for j in range(1, ep):
         relay(j)
     for step in range(1, ep):
@@ -685,6 +684,7 @@
     for e in range(local):
         gacc_s[e] = mm(xw_s[...], wg_v[e, weights_of(0), :])
         uacc_s[e] = mm(xw_s[...], wu_v[e, weights_of(0), :])
+    outputs()
     for step in range(1, chips - 1):
         mates(step)
         gained(step)

time: 35.7 us -> 35.3 us (0.989)
    pallas_call x1, Pallas kernels: 33.8 us -> 33.5 us  [fused_body(): pl.pallas_call(layer_kernel, out_shape=(pltpu.VMEM((length * heads, width...]
where the time goes in v4:
time: 35.3 us; the launch traced here: 35.2 us
  Pallas kernels  34.4 us (97%)
  between operations  0.8 us (2%)
    pallas_call x1, Pallas kernels, fused_body(): pl.pallas_call(layer_kernel, out_shape=(pltpu.VMEM((length * heads, width...  33.5 us
    pallas_call x1, Pallas kernels, fused_body(): pl.pallas_call(hand_on, out_shape=(jax.ShapeDtypeStruct(mix_out.shape, BF...  0.89 us

profile of v4, /device:TPU:0, one launch (start us, length us, event | category | flops | bytes accessed | tf_op | source)
XLA Modules:
  0.0 35.2 jit_solution(6957189513825309111)
XLA Ops:
  0.6 33.5 %shard_map.140 = (bf16[2048,128]{1,0:T(8,128)(2,1)S(1)}, bf16[128,1024]{1,0:T(8,128)(2,1)S(1)}) custom-call(bf16[2048,128]{1,0:T(8,128)(2,1)} %bitcast.8, bf16[2048,128]{1,0:T(8,128)(2,1)} %bitcast.9, bf16[2048,128]{1,0:T(8,128)(2,1)} %bitcast.10, f32[4,512]{1,0:T(4,128)} %beta_hbm.1, f32[4,512]{1,0:T(4,128)} %decay_hbm.1, f32[1,128]{1,0:T(1,128)} %bitcast.14, ...), custom_call_target="tpu_custom_call" | custom-call | tf_op jit(solution)/shard_map/pallas_call | solution.py:831
  34.1 0.9 %shard_map.141 = (bf16[2048,128]{1,0:T(8,128)(2,1)}, bf16[128,1024]{1,0:T(8,128)(2,1)}) custom-call(bf16[2048,128]{1,0:T(8,128)(2,1)S(1)} %get-tuple-element.6.mix_ref, bf16[128,1024]{1,0:T(8,128)(2,1)S(1)} %get-tuple-element.7.ffn_ref), custom_call_target="tpu_custom_call" | custom-call | flops 1000 | bytes 2097152 | tf_op jit(solution)/shard_map/pallas_call | solution.py:909
